TPU v7x, 32 devices: a whole 2x2x4 slice. The times are simulated.
32 devices in a mesh: ep: 8 (over z, y), tp: 4 (over x, core).
Axes of the slice: x: 2, y: 2, z: 4, core: 2. Of those that a mesh axis runs over, the one named last changes fastest.
Arguments:
- att_queries: bfloat16 [8192, 1024], P(('ep', 'tp')), may hold values from -8 to 8
- att_keys: bfloat16 [8192, 256], P(('ep', 'tp')), may hold values from -6 to 6
- att_values: bfloat16 [8192, 256], P(('ep', 'tp')), may hold values from -6 to 6
- sink_logits: float32 [16], replicated, may hold values from 3 to 6.5
- out_weight: bfloat16 [1024, 2048], replicated, may hold values from -0.1875 to 0.1875
- att_gain: float32 [2048], replicated, may hold values from 0.1 to 1.9
- moe_in: bfloat16 [4096, 2048], P(('ep', 'tp')), may hold values from -6 to 6
- pre_gain: float32 [2048], replicated, may hold values from 0.1 to 1.9
- expert_ids: int32 [4096, 2], P(('ep', 'tp')), may hold values from 0 to 15, all different within a row; in each aligned block of 128 rows (0 to 127, 128 to 255, ...) at most 32 rows name the same one
- routed_expert_weight: float32 [4096, 2], P(('ep', 'tp')), may hold values from 0.2 to 1.5
- w_gate: bfloat16 [16, 2048, 768], P('ep', None, 'tp'), may hold values from -0.125 to 0.125
- w_up: bfloat16 [16, 2048, 768], P('ep', None, 'tp'), may hold values from -0.125 to 0.125
- w_down: bfloat16 [16, 768, 2048], P('ep', 'tp'), may hold values from -0.21875 to 0.21875
- common_expert_gate_weight: bfloat16 [2048, 512], P(None, 'tp'), may hold values from -0.125 to 0.125
- common_expert_up_weight: bfloat16 [2048, 512], P(None, 'tp'), may hold values from -0.125 to 0.125
- common_expert_down_weight: bfloat16 [512, 2048], P('tp'), may hold values from -0.25 to 0.25
- moe_gain: float32 [2048], replicated, may hold values from 0.1 to 1.9
Outputs:
- mixer_out: bfloat16 [8192, 2048], P(('ep', 'tp'))
- experts_out: bfloat16 [4096, 2048], P(('ep', 'tp'))
Inputs may be any that keep to these rules, and one draw needn't show every extreme that they name: `expert_ids`: each row names 2 different experts; within the rows of one device no expert is named more than 32 times, and in every draw some expert is named exactly 32 times by the rows of some device.
All inputs are finite; a program needn't handle non-finite values.
Results may differ from a plain program's by a relative error of at most 0.012.
Values may be sent and summed in bfloat16 or wider, within the bound.
No kernel may reach another device: no remote copies, remote signals or barrier semaphores. Data moves between devices by JAX's collectives and lax.ppermute only.
A program may use at most 128 MiB of HBM per device.

v0:
```python
import math

import jax
import jax.numpy as jnp
from jax import lax
from jax.sharding import PartitionSpec as P

HEADS = 16
KV_HEADS = 4
HEAD_DIM = 64
WINDOW = 128


EPS = 1e-06
NEGATIVE = -1e30


def from_behind(block, axis, distance):
    devices = range(lax.axis_size(axis))
    route = [(i - distance, i) for i in devices if i - distance in devices]
    return lax.ppermute(block, axis, route)


def rms_scale(inputs, gain_vec):
    mean_sq = jnp.mean(inputs * inputs, axis=-1, keepdims=True)
    return inputs * lax.rsqrt(mean_sq + EPS) * gain_vec


def slot_table(route_ids, slot_cap):
    flat_ids = route_ids.reshape(-1)
    assigned = flat_ids.shape[0]
    earlier = jnp.arange(assigned)[None, :] < jnp.arange(assigned)[:, None]
    position = jnp.sum((flat_ids[:, None] == flat_ids[None, :]) & earlier, axis=1)
    return (flat_ids * slot_cap + position).reshape(route_ids.shape)


def pack_rows(token_rows, slot_ids, slot_total):
    numbers = jnp.arange(slot_total, dtype=jnp.int32)
    chosen = jnp.any(slot_ids[None, :, :] == numbers[:, None, None], axis=2).astype(jnp.bfloat16)
    return jnp.dot(chosen, token_rows, preferred_element_type=jnp.float32).astype(jnp.bfloat16)


def body(
    att_queries,
    att_keys,
    att_values,
    sink_logits,
    out_weight,
    att_gain,
    moe_in,
    pre_gain,
    expert_ids,
    routed_expert_weight,
    w_gate,
    w_up,
    w_down,
    common_expert_gate_weight,
    common_expert_up_weight,
    common_expert_down_weight,
    moe_gain,
):
    tok_rows = att_queries.shape[0]
    group_size = HEADS // KV_HEADS
    blocks = tok_rows // WINDOW
    kv_rows = jnp.stack([att_keys, att_values])
    rim_rows = from_behind(kv_rows[:, tok_rows - WINDOW :], ("ep", "tp"), 1)
    kv_all = jnp.concatenate([rim_rows, kv_rows], axis=1).reshape(
        2, blocks + 1, WINDOW, KV_HEADS, HEAD_DIM
    )
    kv_band = jnp.concatenate([kv_all[:, :-1], kv_all[:, 1:]], axis=2)
    query_blocks = att_queries.reshape(blocks, WINDOW, KV_HEADS, group_size, HEAD_DIM)
    scores = jnp.einsum(
        "nqgjd,nkgd->ngjqk", query_blocks, kv_band[0], preferred_element_type=jnp.float32
    ) * (1.0 / math.sqrt(HEAD_DIM))
    distance = jnp.arange(WINDOW)[:, None] + WINDOW - jnp.arange(2 * WINDOW)[None, :]
    inside = (distance >= 0) & (distance < WINDOW)
    first_pos = lax.axis_index(("ep", "tp")) * tok_rows
    key_pos = (
        first_pos + jnp.arange(blocks)[:, None] * WINDOW - WINDOW + jnp.arange(2 * WINDOW)[None, :]
    )
    is_valid = inside[None] & (key_pos >= 0)[:, None, :]
    scores = jnp.where(is_valid[:, None, None], scores, NEGATIVE)
    sink_grid = sink_logits.reshape(KV_HEADS, group_size)[None, :, :, None, None]
    row_top = jnp.maximum(jnp.max(scores, axis=-1, keepdims=True), sink_grid)
    exp_scores = jnp.exp(scores - row_top)
    denominator = jnp.sum(exp_scores, axis=-1, keepdims=True) + jnp.exp(sink_grid - row_top)
    probs = (exp_scores / denominator).astype(jnp.bfloat16)
    head_mix = jnp.einsum(
        "ngjqk,nkgd->nqgjd", probs, kv_band[1], preferred_element_type=jnp.float32
    )
    head_mix = head_mix.astype(jnp.bfloat16).reshape(tok_rows, HEADS * HEAD_DIM)
    projected = jnp.dot(head_mix, out_weight, preferred_element_type=jnp.float32)
    mixer_out = rms_scale(projected, att_gain).astype(jnp.bfloat16)
    tokens = moe_in.shape[0]
    top_count = expert_ids.shape[1]
    local_experts = w_gate.shape[0]
    ep_size = lax.axis_size("ep")
    tp_size = lax.axis_size("tp")
    experts = local_experts * ep_size
    slot_cap = 2 * tokens * top_count // experts
    slot_total = experts * slot_cap
    normed = rms_scale(moe_in.astype(jnp.float32), pre_gain).astype(jnp.bfloat16)
    own_slots = slot_table(expert_ids, slot_cap)
    packed = pack_rows(normed, own_slots, slot_total)[None]
    arrived = lax.all_to_all(packed, "ep", split_axis=1, concat_axis=1, tiled=True)
    arrived_all, tokens_all = (
        lax.all_gather(arrived[0], "tp", axis=0, tiled=True),
        lax.all_gather(normed, "tp", axis=0, tiled=True),
    )
    arrived = arrived_all.reshape(tp_size, slot_total, normed.shape[1])
    token_block = tokens_all.reshape(tp_size, tokens, normed.shape[1])
    routed = arrived
    routed = routed.reshape(
        1 * lax.axis_size("tp"), ep_size, local_experts, slot_cap, normed.shape[1]
    )
    gate_act = jnp.einsum("tsjcd,jdf->tsjcf", routed, w_gate, preferred_element_type=jnp.float32)
    up_act = jnp.einsum("tsjcd,jdf->tsjcf", routed, w_up, preferred_element_type=jnp.float32)
    hidden = (jax.nn.silu(gate_act) * up_act).astype(jnp.bfloat16)
    routed_part = jnp.einsum("tsjcf,jfd->tsjcd", hidden, w_down, preferred_element_type=jnp.float32)
    routed_part = routed_part.reshape(1 * lax.axis_size("tp"), slot_total, normed.shape[1])
    common_gate_activation = jnp.einsum(
        "spz,zv->spv", token_block, common_expert_gate_weight, preferred_element_type=jnp.float32
    )
    shared_up_act = jnp.einsum(
        "spz,zv->spv", token_block, common_expert_up_weight, preferred_element_type=jnp.float32
    )
    common_expert_hidden = (jax.nn.silu(common_gate_activation) * shared_up_act).astype(
        jnp.bfloat16
    )
    shared_part = jnp.einsum(
        "nsq,ql->nsl",
        common_expert_hidden,
        common_expert_down_weight,
        preferred_element_type=jnp.float32,
    )
    summed = lax.psum_scatter(
        jnp.concatenate([routed_part, shared_part], axis=1).astype(jnp.bfloat16),
        "tp",
        scatter_dimension=0,
        tiled=True,
    ).astype(jnp.float32)
    routed_out = summed[0, :slot_total].astype(jnp.bfloat16)
    shared_sum = summed[0, slot_total:]
    returned = lax.all_to_all(routed_out, "ep", split_axis=0, concat_axis=0, tiled=True)
    picked = returned[own_slots.reshape(-1)].reshape(tokens, top_count, normed.shape[1])
    combined = (
        jnp.sum(routed_expert_weight[:, :, None] * picked.astype(jnp.float32), axis=1) + shared_sum
    )
    experts_out = rms_scale(combined, moe_gain).astype(jnp.bfloat16)
    return (mixer_out, experts_out)


def solution(mesh):
    in_specs = (
        P(("ep", "tp"), None),
        P(("ep", "tp"), None),
        P(("ep", "tp"), None),
        P(),
        P(),
        P(),
        P(("ep", "tp"), None),
        P(),
        P(("ep", "tp"), None),
        P(("ep", "tp"), None),
        P("ep", None, "tp"),
        P("ep", None, "tp"),
        P("ep", "tp", None),
        P(None, "tp"),
        P(None, "tp"),
        P("tp", None),
        P(),
    )
    out_specs = (P(("ep", "tp"), None), P(("ep", "tp"), None))
    return jax.shard_map(body, mesh=mesh, in_specs=in_specs, out_specs=out_specs, check_vma=False)
```

profile of v0, /device:TPU:0, one launch (start us, length us, event | category | flops | bytes accessed | tf_op | source)
XLA Modules:
  0.0 362.7 jit_solution(12713361354934625359)
XLA Ops:
  7.2 0.9 copy.71
  8.1 0.1 eq.28
  8.2 0.2 convert_reduce_fusion
  8.4 0.1 reduce_sum.61
  8.6 0.1 copy.73
  8.6 0.1 fusion.37
  8.7 1.2 fusion.23
  10.0 1.2 fusion.25
  11.2 0.7 fusion.6
  11.9 5.2 %copy.111 = bf16[1,512,2048]{2,0,1:T(2,128)(2,1)} copy(bf16[1,512,2048]{2,1,0:T(8,128)(2,1)S(1)} %fusion.6) | data formatting | bytes 4194304 | tf_op jit(solution)/shard_map/broadcast_in_dim | solution.py:104
  17.1 0.5 broadcast.169
  17.6 14.5 %reduce = bf16[512,2048]{1,0:T(8,128)(2,1)} reduce(bf16[512,1,2048]{2,1,0:T(2,128)(2,1)} %bitcast.116, bf16[]{:T(256)} %broadcast.169), dimensions={1}, to_apply=%bitcast.113.reduce_sub_computation | reduce | bytes 4194306
  32.1 6.3 %reshape.191 = bf16[8,2,65536]{2,1,0:T(2,128)(2,1)} reshape(bf16[512,2048]{1,0:T(8,128)(2,1)} %reduce) | data formatting | bytes 4194304
  38.4 7.3 %all-to-all-start = ((bf16[8,2,65536]{2,1,0:T(2,128)(2,1)}), bf16[8,2,65536]{2,1,0:T(2,128)(2,1)}, u32[]{:S(2)}, u32[]{:S(2)}) async-start(bf16[8,2,65536]{2,1,0:T(2,128)(2,1)} %reshape.191), calls=%async_computation | async-start | bytes 4194304 | tf_op jit(solution)/shard_map/all_to_all | solution.py:105
  45.7 0.0 all-gather.4.cloned.1.call-start
  45.8 0.7 all-gather.4.cloned.1.call-update
  46.4 0.0 all-gather.6.cloned.1.call-start
  46.5 47.6 %all-to-all-done = bf16[8,2,65536]{2,1,0:T(2,128)(2,1)} async-done(((bf16[8,2,65536]{2,1,0:T(2,128)(2,1)}), bf16[8,2,65536]{2,1,0:T(2,128)(2,1)}, u32[]{:S(2)}, u32[]{:S(2)}) %all-to-all-start) | async-done | bytes 2097184 | tf_op jit(solution)/shard_map/all_to_all | solution.py:105
  94.1 6.8 %reshape.192 = bf16[512,1,2048]{2,1,0:T(2,128)(2,1)} reshape(bf16[8,2,65536]{2,1,0:T(2,128)(2,1)} %all-to-all-done) | data formatting | bytes 4194304
  100.8 4.8 %copy.75 = bf16[1,512,2048]{2,1,0:T(8,128)(2,1)} copy(bf16[1,512,2048]{2,0,1:T(2,128)(2,1)} %bitcast.117) | data formatting | bytes 4194304 | tf_op jit(solution)/shard_map/all_to_all | solution.py:105
  105.6 0.0 all-gather.6.cloned.1.call-update
  105.6 0.2 reduce-scatter.2.cloned.1.call-start
  105.8 0.0 all-gather.4.cloned.1.call-done
  105.9 0.8 copy-done.7
  106.6 2.3 fusion.35
  108.9 5.2 %convolution_convert_fusion = bf16[4,128,2048]{2,1,0:T(8,128)(2,1)} fusion(bf16[4,128,2048]{2,1,0:T(8,128)(2,1)} %bitcast.120, bf16[128,2048]{1,0:T(8,128)(2,1)S(1)} %copy-done.8, bf16[2048,128]{1,0:T(8,128)(2,1)S(1)} %copy-done.9, f32[4,128,128]{2,1,0:T(8,128)S(1)} %fusion.35), kind=kOutput, calls=%fused_computation.12 | convolution fusion | flops 538312704 | bytes 5505024 | tf_op jit(solution)/shard_map/nsq,ql->nsl/dot_general | solution.py:130
  114.2 48.9 %all-gather.6.cloned.1.call-done = bf16[1,2048,2048]{2,1,0:T(8,128)(2,1)} async-done(((bf16[1,512,2048]{2,1,0:T(8,128)(2,1)}), bf16[1,2048,2048]{2,1,0:T(8,128)(2,1)}) %all-gather.6.cloned.1.call-update) | async-done | bytes 8388624 | tf_op jit(solution)/shard_map/all_gather | solution.py:107
  163.1 7.6 %fusion.2 = f32[2,4,8,32,192]{4,3,2,1,0:T(8,128)} fusion(bf16[4,8,2,32,2048]{4,3,2,1,0:T(8,128)(2,1)} %bitcast.128, bf16[2,2048,192]{1,2,0:T(8,128)(2,1)} %param.27), kind=kOutput, calls=%fused_computation.5 | convolution fusion | flops 1610612736 | bytes 11534336 | tf_op jit(solution)/shard_map/tsjcd,jdf->tsjcf/dot_general | solution.py:116
  170.7 13.2 %convert_bitcast_fusion = bf16[4,8,2,32,2048]{4,3,1,0,2:T(8,128)(2,1)} fusion(f32[2,4,8,32,192]{4,3,2,1,0:T(8,128)} %fusion.2, bf16[4,8,2,32,2048]{4,3,2,1,0:T(8,128)(2,1)} %bitcast.129, bf16[2,192,2048]{2,1,0:T(8,128)(2,1)S(1)} %copy-done, bf16[2,2048,192]{1,2,0:T(8,128)(2,1)S(1)} %copy-done.15), kind=kOutput, calls=%fused_computation.2 | convolution fusion | flops 3227779072 | bytes 21495808 | tf_op jit(solution)/shard_map/tsjcf,jfd->tsjcd/dot_general | solution.py:119
  183.8 8.4 %copy.78 = bf16[4,8,2,32,2048]{4,3,2,1,0:T(8,128)(2,1)} copy(bf16[4,8,2,32,2048]{4,3,1,0,2:T(8,128)(2,1)} %convert_bitcast_fusion) | data formatting | bytes 16777216 | tf_op jit(solution)/shard_map/tsjcf,jfd->tsjcd/transpose | solution.py:119
  192.3 10.5 %pad_maximum_fusion = bf16[4,640,2048]{2,1,0:T(8,128)(2,1)} fusion(bf16[4,128,2048]{2,1,0:T(8,128)(2,1)S(1)} %copy-done.2, bf16[4,512,2048]{2,1,0:T(8,128)(2,1)} %bitcast.115), kind=kLoop, calls=%fused_computation.1 | loop fusion | flops 20971520 | bytes 20971520 | tf_op jit(solution)/shard_map/concatenate | solution.py:137
  202.7 0.0 reduce-scatter.2.cloned.1.call-update
  202.7 0.9 copy-done.5
  203.6 0.1 copy-done.6
  203.7 2.8 collective-permute-start
  206.5 0.1 mul.143
  206.7 0.1 add_compare_fusion
  206.8 0.1 broadcast_and_fusion
  206.9 80.4 %reduce-scatter.2.cloned.1.call-done = bf16[1,640,2048]{2,1,0:T(8,128)(2,1)} async-done(((bf16[4,640,2048]{2,1,0:T(8,128)(2,1)}), bf16[1,640,2048]{2,1,0:T(8,128)(2,1)}) %reduce-scatter.2.cloned.1.call-update) | async-done | bytes 2621456 | tf_op jit(solution)/shard_map/reduce_scatter | solution.py:136
  287.3 3.2 slice.36
  290.5 5.6 %all-to-all-start.1 = ((bf16[8,64,2048]{2,1,0:T(8,128)(2,1)}), bf16[8,64,2048]{2,1,0:T(8,128)(2,1)S(1)}, u32[]{:S(2)}, u32[]{:S(2)}) async-start(bf16[8,64,2048]{2,1,0:T(8,128)(2,1)} %bitcast.118), calls=%async_computation.2 | async-start | bytes 4194304 | tf_op jit(solution)/shard_map/all_to_all | solution.py:144
  296.1 1.6 reshape.189
  297.8 0.1 max.18
  297.9 0.1 copy.70
  298.0 0.9 maximum_maximum_fusion
  298.9 0.3 reshape.190
  299.2 1.2 fusion.61
  300.4 1.3 copy.89
  301.7 0.3 copy.90
  301.9 2.1 fusion.5
  304.1 0.1 broadcast_maximum_fusion
  304.2 1.0 fusion.4
  305.1 0.1 exponential_add_fusion
  305.2 1.2 fusion.21
  306.4 0.5 copy.69
  307.0 0.4 copy-done.14
  307.4 1.4 multiply_reduce_fusion.1
  308.8 1.2 multiply_convert_fusion
  310.0 34.2 %all-to-all-done.1 = bf16[8,64,2048]{2,1,0:T(8,128)(2,1)S(1)} async-done(((bf16[8,64,2048]{2,1,0:T(8,128)(2,1)}), bf16[8,64,2048]{2,1,0:T(8,128)(2,1)S(1)}, u32[]{:S(2)}, u32[]{:S(2)}) %all-to-all-start.1) | async-done | bytes 2097184 | tf_op jit(solution)/shard_map/all_to_all | solution.py:144
  344.2 1.4 gather_fusion
  345.6 2.3 reshape.169
  347.9 4.9 %multiply_reduce_fusion = f32[128,2048]{1,0:T(8,128)S(1)} fusion(f32[128,2,2048]{2,1,0:T(2,128)} %reshape.169, f32[128,2]{1,0:T(8,128)S(1)} %copy.70), kind=kLoop, calls=%fused_computation.22 | loop fusion | flops 786432 | bytes 3146752 | tf_op jit(solution)/shard_map/reduce_sum | solution.py:147
  352.9 1.3 multiply_reduce_fusion.2
  354.2 2.0 multiply_convert_fusion.1
  (39 shorter events, 0.2 us)
Async XLA Ops:
  7.2 163.5 %copy-start = (bf16[2,192,2048]{2,1,0:T(8,128)(2,1)S(1)}, bf16[2,192,2048]{2,1,0:T(8,128)(2,1)}, u32[]{:S(2)}) copy-start(bf16[2,192,2048]{2,1,0:T(8,128)(2,1)} %param.29) | copy-start | bytes 4718596
  11.2 5.9 %copy-start.3 = (bf16[128,2048]{1,0:T(8,128)(2,1)}, bf16[128,2048]{1,0:T(8,128)(2,1)S(1)}, u32[]{:S(2)}) copy-start(bf16[128,2048]{1,0:T(8,128)(2,1)S(1)} %fusion.25) | copy-start | bytes 1572868
  38.4 55.7 %all-to-all-start = ((bf16[8,2,65536]{2,1,0:T(2,128)(2,1)}), bf16[8,2,65536]{2,1,0:T(2,128)(2,1)}, u32[]{:S(2)}, u32[]{:S(2)}) async-start(bf16[8,2,65536]{2,1,0:T(2,128)(2,1)} %reshape.191), calls=%async_computation | async-start | bytes 4194304 | tf_op jit(solution)/shard_map/all_to_all | solution.py:105
  45.7 60.1 %all-gather.4.cloned.1.call-start = ((), (), s32[]{:S(2)}) async-start(), calls=%async_computation.3 | async-start | bytes 2621440 | tf_op jit(solution)/shard_map/all_gather | solution.py:108
  46.4 116.6 %all-gather.6.cloned.1.call-start = ((), (), s32[]{:S(2)}) async-start(), calls=%async_computation.5 | async-start | bytes 10485760 | tf_op jit(solution)/shard_map/all_gather | solution.py:107
  105.6 1.0 copy-start.7
  105.6 3.3 copy-start.8
  105.6 3.3 copy-start.9
  105.6 181.7 %reduce-scatter.2.cloned.1.call-start = ((), (), s32[]{:S(2)}) async-start(), calls=%async_computation.4 | async-start | bytes 13107200 | tf_op jit(solution)/shard_map/reduce_scatter | solution.py:136
  163.1 7.6 %copy-start.15 = (bf16[2,2048,192]{1,2,0:T(8,128)(2,1)S(1)}, bf16[2,2048,192]{1,2,0:T(8,128)(2,1)}, u32[]{:S(2)}) copy-start(bf16[2,2048,192]{1,2,0:T(8,128)(2,1)} %param.28) | copy-start | bytes 4718596
  183.8 8.4 %copy-start.2 = (bf16[4,128,2048]{2,1,0:T(8,128)(2,1)S(1)}, bf16[4,128,2048]{2,1,0:T(8,128)(2,1)}, u32[]{:S(2)}) copy-start(bf16[4,128,2048]{2,1,0:T(8,128)(2,1)} %convolution_convert_fusion) | copy-start | bytes 6291460
  202.7 0.9 copy-start.5
  202.7 1.0 copy-start.6
  203.7 94.3 %collective-permute-start = (bf16[2,128,256]{2,1,0:T(8,128)(2,1)S(1)}, bf16[2,128,256]{2,1,0:T(8,128)(2,1)}, u32[]{:S(2)}, u32[]{:S(2)}) collective-permute-start(bf16[2,128,256]{2,1,0:T(8,128)(2,1)S(1)} %pad_maximum_fusion.2), channel_id=1, source_target_pairs={{0,1},{1,2},{2,3},{3,4},{4,5},{5,6},{6,7},{7,8},{8,9},{9,10},{10,1... | collective-permute-start | bytes 393224 | tf_op jit(solution)/shard_map/ppermute | solution.py:21
  290.5 5.7 %copy-start.4 = (bf16[256,1024]{1,0:T(8,128)(2,1)S(1)}, bf16[256,1024]{1,0:T(8,128)(2,1)}, u32[]{:S(2)}) copy-start(bf16[256,1024]{1,0:T(8,128)(2,1)} %param.17) | copy-start | bytes 1572868
  290.5 7.3 %copy-start.13 = (f32[16]{0:T(128)S(1)}, f32[16]{0:T(128)}, u32[]{:S(2)}) copy-start(f32[16]{0:T(128)} %param.20) | copy-start | bytes 196
  290.5 7.4 %copy-start.12 = (f32[128,2]{0,1:T(2,128)S(1)}, f32[128,2]{0,1:T(2,128)}, u32[]{:S(2)}) copy-start(f32[128,2]{0,1:T(2,128)} %param.26) | copy-start | bytes 3076
  290.5 53.7 %all-to-all-start.1 = ((bf16[8,64,2048]{2,1,0:T(8,128)(2,1)}), bf16[8,64,2048]{2,1,0:T(8,128)(2,1)S(1)}, u32[]{:S(2)}, u32[]{:S(2)}) async-start(bf16[8,64,2048]{2,1,0:T(8,128)(2,1)} %bitcast.118), calls=%async_computation.2 | async-start | bytes 4194304 | tf_op jit(solution)/shard_map/all_to_all | solution.py:144
  305.2 2.2 copy-start.14
  307.4 1.4 copy-start.10
  347.9 6.2 %copy-start.11 = (f32[2048]{0:T(1024)S(1)}, f32[2048]{0:T(1024)}, u32[]{:S(2)}) copy-start(f32[2048]{0:T(1024)} %param.33) | copy-start | bytes 24580
  347.9 8.3 %copy-start.1 = (bf16[2,192,2048]{2,1,0:T(8,128)(2,1)S(1)}, bf16[2,192,2048]{2,1,0:T(8,128)(2,1)}, u32[]{:S(2)}) copy-start(bf16[2,192,2048]{2,1,0:T(8,128)(2,1)} %param.29) | copy-start | bytes 4718596
Sparse Core Ops, SparseCore 0:
  48.7 23.9 all-gather.3
  105.7 57.2 all-gather.5
  202.9 84.3 reduce-scatter.1
where the time goes:
time: 364 us; the launch traced here: 363 us
  waiting for transfers between devices  212 us (58%)
  local copies, waits for them, and re-layouts  47.7 us (13%)
  other arithmetic  39.5 us (11%)
  matrix products  33.7 us (9%)
  starting transfers between devices  16.1 us (4%)
  between operations  14 us (4%)
    reduce_scatter x1, waiting for transfers between devices, body(): lax.psum_scatter(jnp.concatenate([routed_part, shared_part], axis=1).asty...  80.4 us
    all_gather x1, waiting for transfers between devices, body(): lax.all_gather(arrived[0], 'tp', axis=0, tiled=True)  48.9 us
    all_to_all x1, waiting for transfers between devices, body(): lax.all_to_all(packed, 'ep', split_axis=1, concat_axis=1, tiled=True)  47.6 us
    all_to_all x1, waiting for transfers between devices, body(): lax.all_to_all(routed_out, 'ep', split_axis=0, concat_axis=0, tiled=True)  34.2 us
    unnamed x39, local copies, waits for them, and re-layouts  18.3 us
    unnamed x1, other arithmetic  14.5 us
    dot_general x1, matrix products, body(): jnp.einsum('tsjcf,jfd->tsjcd', hidden, w_down, preferred_element_type=jnp...  13.2 us
    concatenate x1, other arithmetic, body(): jnp.concatenate([routed_part, shared_part], axis=1).astype(jnp.bfloat16)  10.5 us
  transfers between devices with their start and end apart: 6, of which 4 were waited for; matrix products, arithmetic and copies ran while one was open for 10% of the time, Pallas kernels for 0%

commit v1 on v0

--- a/solution.py
+++ b/solution.py
@@ -1,8 +1,11 @@
+import functools
 import math
 
 import jax
 import jax.numpy as jnp
 from jax import lax
+from jax.experimental import pallas as pl
+from jax.experimental.pallas import tpu as pltpu
 from jax.sharding import PartitionSpec as P
 
 HEADS = 16
@@ -13,6 +16,8 @@
 
 EPS = 1e-06
 NEGATIVE = -1e30
+NEAR_LIMIT = 8
+KERNEL_VMEM = 24 * 1024 * 1024
 
 
 def from_behind(block, axis, distance):
@@ -40,13 +45,80 @@
     return jnp.dot(chosen, token_rows, preferred_element_type=jnp.float32).astype(jnp.bfloat16)
 
 
-def body(
-    att_queries,
-    att_keys,
-    att_values,
-    sink_logits,
-    out_weight,
-    att_gain,
+def attention_kernel(q_ref, k_ref, v_ref, rim_ref, sink_ref, first_ref, weight_ref, gain_ref, out_ref, mix_ref):
+    lanes = 2 * HEAD_DIM
+    group_size = HEADS // KV_HEADS
+    blocks = q_ref.shape[0] // WINDOW
+    query = lax.broadcasted_iota(jnp.int32, (WINDOW, 2 * WINDOW), 0)
+    key = lax.broadcasted_iota(jnp.int32, (WINDOW, 2 * WINDOW), 1)
+    inside = (key > query) & (key <= query + WINDOW)
+    low = lax.broadcasted_iota(jnp.int32, (2 * WINDOW, lanes), 1) < HEAD_DIM
+
+    def spread(tile, group):
+        tile = tile.astype(jnp.float32)
+        kept = jnp.where(low if group % 2 == 0 else ~low, tile, 0.0)
+        moved = pltpu.roll(kept, HEAD_DIM, 1)
+        both = [kept, moved] if group % 2 == 0 else [moved, kept]
+        return jnp.concatenate(both, axis=0).astype(jnp.bfloat16)
+
+    for block in range(blocks):
+        at = slice(block * WINDOW, (block + 1) * WINDOW)
+        before = slice((block - 1) * WINDOW, block * WINDOW)
+        valid = inside
+        if block == 0:
+            valid = inside & (key >= first_ref[0] * WINDOW)
+        for tile in range(KV_HEADS // 2):
+            span = slice(tile * lanes, (tile + 1) * lanes)
+            earlier_k = rim_ref[0, :, span] if block == 0 else k_ref[before, span]
+            earlier_v = rim_ref[1, :, span] if block == 0 else v_ref[before, span]
+            band_k = jnp.concatenate([earlier_k, k_ref[at, span]], axis=0)
+            band_v = jnp.concatenate([earlier_v, v_ref[at, span]], axis=0)
+            for group in (2 * tile, 2 * tile + 1):
+                keys, values = spread(band_k, group), spread(band_v, group)
+                for pair in range(group * group_size // 2, (group + 1) * group_size // 2):
+                    cols = slice(pair * lanes, (pair + 1) * lanes)
+                    scores = dot_last(q_ref[at, cols], keys) * (1.0 / math.sqrt(HEAD_DIM))
+                    probs = []
+                    for part in range(2):
+                        sink = sink_ref[2 * pair + part]
+                        own = scores[:, part * 2 * WINDOW : (part + 1) * 2 * WINDOW]
+                        own = jnp.where(valid, own, NEGATIVE)
+                        row_top = jnp.maximum(jnp.max(own, axis=-1, keepdims=True), sink)
+                        grown = jnp.exp(own - row_top)
+                        total = jnp.sum(grown, axis=-1, keepdims=True) + jnp.exp(sink - row_top)
+                        probs.append((grown * (1.0 / total)).astype(jnp.bfloat16))
+                    mixed = jnp.dot(
+                        jnp.concatenate(probs, axis=1), values, preferred_element_type=jnp.float32
+                    )
+                    mix_ref[at, cols] = mixed.astype(jnp.bfloat16)
+    projected = jnp.dot(mix_ref[...], weight_ref[...], preferred_element_type=jnp.float32)
+    mean_sq = jnp.mean(projected * projected, axis=-1, keepdims=True)
+    out_ref[...] = (projected * lax.rsqrt(mean_sq + EPS) * gain_ref[...]).astype(jnp.bfloat16)
+
+
+def attention(att_queries, att_keys, att_values, sink_logits, out_weight, att_gain):
+    rows, columns = att_queries.shape
+    width = out_weight.shape[1]
+    last = slice(rows - WINDOW, rows)
+    rim = from_behind(jnp.stack([att_keys[last], att_values[last]]), ("ep", "tp"), 1)
+    first = (lax.axis_index(("ep", "tp")) == 0).astype(jnp.int32)[None]
+    inner, scalars = pl.BlockSpec(memory_space=pltpu.VMEM), pl.BlockSpec(memory_space=pltpu.SMEM)
+    return pl.pallas_call(
+        attention_kernel,
+        out_shape=jax.ShapeDtypeStruct((rows, width), jnp.bfloat16),
+        in_specs=[inner] * 4 + [scalars] * 2 + [inner] * 2,
+        out_specs=inner,
+        scratch_shapes=[pltpu.VMEM((rows, columns), jnp.bfloat16)],
+        compiler_params=pltpu.CompilerParams(vmem_limit_bytes=KERNEL_VMEM),
+        cost_estimate=pl.CostEstimate(
+            flops=2 * rows * columns * (width + 8 * WINDOW),
+            bytes_accessed=2 * (rows * columns + columns * width + rows * width),
+            transcendentals=rows * HEADS * 2 * WINDOW,
+        ),
+    )(att_queries, att_keys, att_values, rim, sink_logits, first, out_weight, att_gain[None])
+
+
+def experts_wide(
     moe_in,
     pre_gain,
     expert_ids,
@@ -59,38 +131,6 @@
     common_expert_down_weight,
     moe_gain,
 ):
-    tok_rows = att_queries.shape[0]
-    group_size = HEADS // KV_HEADS
-    blocks = tok_rows // WINDOW
-    kv_rows = jnp.stack([att_keys, att_values])
-    rim_rows = from_behind(kv_rows[:, tok_rows - WINDOW :], ("ep", "tp"), 1)
-    kv_all = jnp.concatenate([rim_rows, kv_rows], axis=1).reshape(
-        2, blocks + 1, WINDOW, KV_HEADS, HEAD_DIM
-    )
-    kv_band = jnp.concatenate([kv_all[:, :-1], kv_all[:, 1:]], axis=2)
-    query_blocks = att_queries.reshape(blocks, WINDOW, KV_HEADS, group_size, HEAD_DIM)
-    scores = jnp.einsum(
-        "nqgjd,nkgd->ngjqk", query_blocks, kv_band[0], preferred_element_type=jnp.float32
-    ) * (1.0 / math.sqrt(HEAD_DIM))
-    distance = jnp.arange(WINDOW)[:, None] + WINDOW - jnp.arange(2 * WINDOW)[None, :]
-    inside = (distance >= 0) & (distance < WINDOW)
-    first_pos = lax.axis_index(("ep", "tp")) * tok_rows
-    key_pos = (
-        first_pos + jnp.arange(blocks)[:, None] * WINDOW - WINDOW + jnp.arange(2 * WINDOW)[None, :]
-    )
-    is_valid = inside[None] & (key_pos >= 0)[:, None, :]
-    scores = jnp.where(is_valid[:, None, None], scores, NEGATIVE)
-    sink_grid = sink_logits.reshape(KV_HEADS, group_size)[None, :, :, None, None]
-    row_top = jnp.maximum(jnp.max(scores, axis=-1, keepdims=True), sink_grid)
-    exp_scores = jnp.exp(scores - row_top)
-    denominator = jnp.sum(exp_scores, axis=-1, keepdims=True) + jnp.exp(sink_grid - row_top)
-    probs = (exp_scores / denominator).astype(jnp.bfloat16)
-    head_mix = jnp.einsum(
-        "ngjqk,nkgd->nqgjd", probs, kv_band[1], preferred_element_type=jnp.float32
-    )
-    head_mix = head_mix.astype(jnp.bfloat16).reshape(tok_rows, HEADS * HEAD_DIM)
-    projected = jnp.dot(head_mix, out_weight, preferred_element_type=jnp.float32)
-    mixer_out = rms_scale(projected, att_gain).astype(jnp.bfloat16)
     tokens = moe_in.shape[0]
     top_count = expert_ids.shape[1]
     local_experts = w_gate.shape[0]
@@ -147,7 +187,250 @@
         jnp.sum(routed_expert_weight[:, :, None] * picked.astype(jnp.float32), axis=1) + shared_sum
     )
     experts_out = rms_scale(combined, moe_gain).astype(jnp.bfloat16)
-    return (mixer_out, experts_out)
+    return experts_out
+
+
+def swap(block, axis, bit):
+    route = [(i, i ^ bit) for i in range(lax.axis_size(axis))]
+    return lax.ppermute(block, axis, route)
+
+
+def dot_last(left, right):
+    return lax.dot_general(
+        left, right, (((1,), (1,)), ((), ())), preferred_element_type=jnp.float32
+    )
+
+
+def gated(gate_act, up_act):
+    return (gate_act / (1.0 + jnp.exp(-gate_act)) * up_act).astype(jnp.bfloat16)
+
+
+def run_kernel(kernel, outs, flops, *operands):
+    size = sum(o.size * o.dtype.itemsize for o in (*operands, *outs))
+    return pl.pallas_call(
+        kernel,
+        out_shape=outs,
+        compiler_params=pltpu.CompilerParams(vmem_limit_bytes=KERNEL_VMEM),
+        cost_estimate=pl.CostEstimate(flops=flops, bytes_accessed=size, transcendentals=0),
+    )(*operands)
+
+
+def prepare_kernel(cap, in_ref, gain_ref, rel_ref, weight_ref, normed_ref, top_ref, rest_ref, near_ref, *pieces):
+    rows = in_ref[...].astype(jnp.float32)
+    mean_sq = jnp.mean(rows * rows, axis=-1, keepdims=True)
+    normed = (rows * lax.rsqrt(mean_sq + EPS) * gain_ref[...]).astype(jnp.bfloat16)
+    normed_ref[...] = normed
+    top_count, tokens = rel_ref.shape
+    piece_rows = pieces[0].shape[0]
+    slots = (1 + len(pieces)) * piece_rows
+    experts = slots // cap
+    expert_row = lax.broadcasted_iota(jnp.int32, (experts, tokens), 0)
+    named = [rel_ref[k : k + 1, :] == expert_row for k in range(top_count)]
+    counts = sum(jnp.where(hit, 1.0, 0.0) for hit in named)
+    before = lax.broadcasted_iota(jnp.int32, (tokens, tokens), 0) < lax.broadcasted_iota(
+        jnp.int32, (tokens, tokens), 1
+    )
+    prior = jnp.dot(
+        counts.astype(jnp.bfloat16),
+        jnp.where(before, 1.0, 0.0).astype(jnp.bfloat16),
+        preferred_element_type=jnp.float32,
+    )
+    slot_row = lax.broadcasted_iota(jnp.int32, (slots, tokens), 0)
+    chosen = jnp.zeros((slots, tokens), jnp.float32)
+    share = jnp.zeros((slots, tokens), jnp.float32)
+    for k, hit in enumerate(named):
+        position = jnp.sum(jnp.where(hit, prior, 0.0), axis=0, keepdims=True)
+        slot = rel_ref[k : k + 1, :] * cap + position.astype(jnp.int32)
+        here = slot == slot_row
+        chosen = chosen + jnp.where(here, 1.0, 0.0)
+        share = share + jnp.where(here, weight_ref[k : k + 1, :], 0.0)
+    chosen = chosen.astype(jnp.bfloat16)
+    for p, piece in enumerate(pieces, 1):
+        piece[...] = jnp.dot(
+            chosen[p * piece_rows : (p + 1) * piece_rows],
+            normed,
+            preferred_element_type=jnp.float32,
+        ).astype(jnp.bfloat16)
+    top = share.astype(jnp.bfloat16)
+    rest = (share - top.astype(jnp.float32)).astype(jnp.bfloat16)
+    top_ref[...] = top[piece_rows:]
+    rest_ref[...] = rest[piece_rows:]
+    near_ref[...] = jnp.concatenate([t[:piece_rows] for t in (chosen, top, rest)], axis=0)
+
+
+def routed(rows, j, gate_a, gate_b, up_a, up_b, down_a, down_b):
+    wide = jnp.concatenate([gate_a[j], gate_b[j], up_a[j], up_b[j]], axis=0)
+    act = dot_last(rows, wide)
+    half = act.shape[1] // 2
+    hidden = gated(act[:, :half], act[:, half:])
+    down = jnp.concatenate([down_a[j], down_b[j]], axis=0)
+    return jnp.dot(hidden, down, preferred_element_type=jnp.float32).astype(jnp.bfloat16)
+
+
+def routed_kernel(cap, count, *refs):
+    pieces, weights, outs = refs[:count], refs[count : count + 6], refs[count + 6 :]
+    for j in range(weights[0].shape[0]):
+        at = slice(j * cap, (j + 1) * cap)
+        rows = jnp.concatenate([piece[at, :] for piece in pieces], axis=0)
+        out = routed(rows, j, *weights)
+        for p, out_ref in enumerate(outs):
+            out_ref[at, :] = out[p * cap : (p + 1) * cap]
+
+
+def local_kernel(cap, own_ref, other_ref, own_tab, other_tab, *refs):
+    ga, gb, ua, ub, da, db = refs[:6]
+    weights, (own_out, other_out) = refs[6:12], refs[12:]
+    tokens = own_ref.shape[0]
+    piece_rows = own_tab.shape[0] // 3
+    rows = jnp.concatenate([own_ref[...], other_ref[...]], axis=0)
+    gate = jnp.concatenate([ga[...], gb[...]], axis=1)
+    up = jnp.concatenate([ua[...], ub[...]], axis=1)
+    down = jnp.concatenate([da[...], db[...]], axis=0)
+    hidden = gated(
+        jnp.dot(rows, gate, preferred_element_type=jnp.float32),
+        jnp.dot(rows, up, preferred_element_type=jnp.float32),
+    )
+    out = jnp.dot(hidden, down, preferred_element_type=jnp.float32)
+    picked = [
+        jnp.dot(tab[:piece_rows], ref[...], preferred_element_type=jnp.float32).astype(jnp.bfloat16)
+        for tab, ref in ((own_tab, own_ref), (other_tab, other_ref))
+    ]
+    parts = [[], []]
+    for j in range(piece_rows // cap):
+        at = slice(j * cap, (j + 1) * cap)
+        part = routed(jnp.concatenate([p[at] for p in picked], axis=0), j, *weights)
+        parts[0].append(part[:cap])
+        parts[1].append(part[cap:])
+    for tab, part, half, out_ref in (
+        (own_tab, parts[0], out[:tokens], own_out),
+        (other_tab, parts[1], out[tokens:], other_out),
+    ):
+        part = jnp.concatenate(part + part, axis=0)
+        share = lax.dot_general(
+            tab[piece_rows:], part, (((0,), (0,)), ((), ())), preferred_element_type=jnp.float32
+        )
+        out_ref[...] = (half + share).astype(out_ref.dtype)
+
+
+def combine_kernel(top_ref, rest_ref, shared_ref, back_ref, gain_ref, *refs):
+    pieces, out_ref = refs[:-1], refs[-1]
+    rows = jnp.concatenate([piece[...] for piece in pieces], axis=0)
+    total = shared_ref[...] + back_ref[...].astype(jnp.float32)
+    for table in (top_ref, rest_ref):
+        total = total + lax.dot_general(
+            table[...], rows, (((0,), (0,)), ((), ())), preferred_element_type=jnp.float32
+        )
+    mean_sq = jnp.mean(total * total, axis=-1, keepdims=True)
+    out_ref[...] = (total * lax.rsqrt(mean_sq + EPS) * gain_ref[...]).astype(jnp.bfloat16)
+
+
+def experts_near(
+    moe_in,
+    pre_gain,
+    expert_ids,
+    routed_expert_weight,
+    w_gate,
+    w_up,
+    w_down,
+    common_expert_gate_weight,
+    common_expert_up_weight,
+    common_expert_down_weight,
+    moe_gain,
+):
+    tokens, width = moe_in.shape
+    top_count = expert_ids.shape[1]
+    local_experts, _, units = w_gate.shape
+    shared_units = common_expert_gate_weight.shape[1]
+    ep_size = lax.axis_size("ep")
+    near_bit, far_bit = 1, lax.axis_size("tp") // 2
+    experts = local_experts * ep_size
+    cap = 2 * tokens * top_count // experts
+    piece_rows = local_experts * cap
+    own = lax.axis_index("ep")
+
+    def array(rows, kind=jnp.bfloat16):
+        return jax.ShapeDtypeStruct((rows, width), kind)
+
+    def paired(block):
+        return block, swap(block, "tp", near_bit)
+
+    weights = (*paired(w_gate.swapaxes(1, 2)), *paired(w_up.swapaxes(1, 2)), *paired(w_down))
+    common = (
+        *paired(common_expert_gate_weight),
+        *paired(common_expert_up_weight),
+        *paired(common_expert_down_weight),
+    )
+    ids = expert_ids.T
+    relative = ((ids // local_experts) ^ own) * local_experts + ids % local_experts
+    far_rows = (ep_size - 1) * piece_rows
+    table = jax.ShapeDtypeStruct((far_rows, tokens), jnp.bfloat16)
+    near_table = jax.ShapeDtypeStruct((3 * piece_rows, tokens), jnp.bfloat16)
+    normed, top, rest, near_tab, *pieces = run_kernel(
+        functools.partial(prepare_kernel, cap),
+        (array(tokens), table, table, near_table) + (array(piece_rows),) * (ep_size - 1),
+        2 * ep_size * piece_rows * tokens * width,
+        moe_in,
+        pre_gain[None],
+        relative,
+        routed_expert_weight.T,
+    )
+    arrived = [None] + [swap(pieces[r - 1], "ep", r) for r in range(1, ep_size)]
+    other_rows = swap(normed, "tp", far_bit)
+    other_tab = swap(near_tab, "tp", far_bit)
+    local_own, local_other = run_kernel(
+        functools.partial(local_kernel, cap),
+        (array(tokens, jnp.float32), array(tokens)),
+        12 * width * (2 * tokens * shared_units + 2 * piece_rows * units),
+        normed,
+        other_rows,
+        near_tab,
+        other_tab,
+        *common,
+        *weights,
+    )
+    local_back = swap(local_other, "tp", far_bit)
+
+    returned = [None] * ep_size
+    for chunk in chunks_of(ep_size):
+        mine = [arrived[r] for r in chunk]
+        other = [swap(arrived[r], "tp", far_bit) for r in chunk]
+        parts = run_kernel(
+            functools.partial(routed_kernel, cap, 2 * len(chunk)),
+            (array(piece_rows),) * (2 * len(chunk)),
+            2 * 2 * len(chunk) * piece_rows * 3 * width * 2 * units,
+            *mine,
+            *other,
+            *weights,
+        )
+        for r, part, sent in zip(chunk, parts, parts[len(chunk) :]):
+            back = swap(sent, "tp", far_bit)
+            total = (part.astype(jnp.float32) + back.astype(jnp.float32)).astype(jnp.bfloat16)
+            returned[r] = swap(total, "ep", r)
+    return run_kernel(
+        combine_kernel,
+        (array(tokens),),
+        2 * 2 * far_rows * tokens * width,
+        top,
+        rest,
+        local_own,
+        local_back,
+        moe_gain[None],
+        *returned[1:],
+    )[0]
+
+
+def chunks_of(ep_size):
+    return [list(range(1, min(4, ep_size)))] + [[r, r + 1] for r in range(4, ep_size, 2)]
+
+
+def is_near(ep_size, tp_size):
+    return ep_size <= NEAR_LIMIT and ep_size & (ep_size - 1) == 0 and tp_size == 4
+
+
+def body(*args):
+    near = is_near(lax.axis_size("ep"), lax.axis_size("tp"))
+    experts_out = (experts_near if near else experts_wide)(*args[6:])
+    return (attention(*args[:6]), experts_out)
 
 
 def solution(mesh):
@@ -171,4 +454,6 @@
         P(),
     )
     out_specs = (P(("ep", "tp"), None), P(("ep", "tp"), None))
-    return jax.shard_map(body, mesh=mesh, in_specs=in_specs, out_specs=out_specs, check_vma=False)
+    return jax.shard_map(
+        body, mesh=mesh, in_specs=in_specs, out_specs=out_specs, check_vma=False
+    )

time: 364 us -> 211 us (0.58)
  waiting for transfers between devices: 212 us -> 93.3 us
  starting transfers between devices: 16.1 us -> 72.7 us
  local copies, waits for them, and re-layouts: 47.7 us -> 9.77 us
  other arithmetic: 39.5 us -> 3.98 us
  matrix products: 33.7 us -> 0 us
  Pallas kernels: 0 us -> 28.9 us
  between operations: 14 us -> 0.91 us
    ppermute x0 -> x37, waiting for transfers between devices: none -> 93.3 us  [swap(): return lax.ppermute(block, axis, route)]
    all_to_all x2 -> x0, waiting for transfers between devices: 81.8 us -> none  [the longest x1 47.6 us: body(): lax.all_to_all(packed, 'ep', split_axis=1, concat_axis=1, tiled=True)]
    reduce_scatter x1 -> x0, waiting for transfers between devices: 80.4 us -> none  [body(): lax.psum_scatter(jnp.concatenate([routed_part, shared_part], axis=1).asty...]
    ppermute x0 -> x37, starting transfers between devices: none -> 71.2 us  [swap(): return lax.ppermute(block, axis, route)]
    all_gather x2 -> x0, waiting for transfers between devices: 48.9 us -> none  [the longest x1 48.9 us: body(): lax.all_gather(arrived[0], 'tp', axis=0, tiled=True)]
    dot_general x8 -> x0, matrix products: 33.7 us -> none  [the longest x1 13.2 us: body(): jnp.einsum('tsjcf,jfd->tsjcd', hidden, w_down, preferred_element_type=jnp...]
    pallas_call x0 -> x7, Pallas kernels: none -> 28.9 us  [the longest x6 19.5 us: run_kernel(): pl.pallas_call(kernel, out_shape=outs, compiler_params=pltpu.CompilerPara...]
    unnamed x1 -> x0, other arithmetic: 14.5 us -> none
  transfers between devices with their start and end apart: 6 -> 38, of which waited for: 4 -> 20; matrix products, arithmetic and copies ran while one was open for 10% -> 2% of each run, Pallas kernels for 0% -> 12%
where the time goes in v1:
time: 211 us; the launch traced here: 210 us
  waiting for transfers between devices  93.3 us (44%)
  starting transfers between devices  72.7 us (34%)
  Pallas kernels  28.9 us (14%)
  local copies, waits for them, and re-layouts  9.77 us (5%)
  other arithmetic  3.98 us (2%)
    ppermute x37, waiting for transfers between devices, swap(): return lax.ppermute(block, axis, route)  93.3 us
    ppermute x37, starting transfers between devices, swap(): return lax.ppermute(block, axis, route)  71.2 us
    pallas_call x6, Pallas kernels, run_kernel(): pl.pallas_call(kernel, out_shape=outs, compiler_params=pltpu.CompilerPara...  19.5 us
    pallas_call x1, Pallas kernels, attention(): pl.pallas_call(attention_kernel, out_shape=jax.ShapeDtypeStruct((rows, wi...  9.41 us
    unnamed x46, local copies, waits for them, and re-layouts  8.89 us
  transfers between devices with their start and end apart: 38, of which 20 were waited for; matrix products, arithmetic and copies ran while one was open for 2% of the time, Pallas kernels for 12%

profile of v1, /device:TPU:0, one launch (start us, length us, event | category | flops | bytes accessed | tf_op | source)
XLA Modules:
  0.0 209.6 jit_solution(4962748163801492545)
XLA Ops:
  0.6 0.7 fusion.rel_ref
  1.3 1.0 copy-done.20
  2.4 0.7 copy-done.21
  3.1 0.7 copy-done.22
  3.8 0.9 shard_map.177
  4.7 3.0 %collective-permute-start.2 = (bf16[192,128]{1,0:T(8,128)(2,1)S(1)}, bf16[192,128]{1,0:T(8,128)(2,1)S(1)}, u32[]{:S(2)}, u32[]{:S(2)}) collective-permute-start(bf16[192,128]{1,0:T(8,128)(2,1)S(1)} %get-tuple-element.32.own_tab), channel_id=1, source_target_pairs={{0,2},{1,3},{2,0},{3,1},{4,6},{5,7},{6,4},{7,5},{8,10},{9,11},{10,... | collective-permute-start | bytes 147464 | tf_op jit(solution)/shard_map/ppermute | solution.py:195
  7.7 1.5 collective-permute-start.10
  9.2 1.6 collective-permute-start.11
  11.7 4.3 %collective-permute-done.10.refs_0_ = bf16[64,2048]{1,0:T(8,128)(2,1)S(1)} collective-permute-done((bf16[64,2048]{1,0:T(8,128)(2,1)S(1)}, bf16[64,2048]{1,0:T(8,128)(2,1)S(1)}, u32[]{:S(2)}, u32[]{:S(2)}) %collective-permute-start.10) | collective-permute-done | bytes 262176 | tf_op jit(solution)/shard_map/ppermute | solution.py:195
  16.0 2.4 %collective-permute-done.11.refs_1_ = bf16[64,2048]{1,0:T(8,128)(2,1)S(1)} collective-permute-done((bf16[64,2048]{1,0:T(8,128)(2,1)S(1)}, bf16[64,2048]{1,0:T(8,128)(2,1)S(1)}, u32[]{:S(2)}, u32[]{:S(2)}) %collective-permute-start.11) | collective-permute-done | bytes 262176 | tf_op jit(solution)/shard_map/ppermute | solution.py:195
  18.4 3.6 %collective-permute-start.30 = (bf16[64,2048]{1,0:T(8,128)(2,1)S(1)}, bf16[64,2048]{1,0:T(8,128)(2,1)S(1)}, u32[]{:S(2)}, u32[]{:S(2)}) collective-permute-start(bf16[64,2048]{1,0:T(8,128)(2,1)S(1)} %get-tuple-element.50), channel_id=1, source_target_pairs={{0,24},{4,28},{8,16},{12,20},{16,8},{20,12},{24,0},{28,4},{1,25},{... | collective-permute-start | bytes 786440 | tf_op jit(solution)/shard_map/ppermute | solution.py:195
  22.0 0.6 collective-permute-done.12.refs_2_
  22.6 12.6 %collective-permute-start.31 = (bf16[64,2048]{1,0:T(8,128)(2,1)S(1)}, bf16[64,2048]{1,0:T(8,128)(2,1)S(1)}, u32[]{:S(2)}, u32[]{:S(2)}) collective-permute-start(bf16[64,2048]{1,0:T(8,128)(2,1)S(1)} %get-tuple-element.51), channel_id=1, source_target_pairs={{0,28},{4,24},{8,20},{12,16},{16,12},{20,8},{24,4},{28,0},{1,29},{... | collective-permute-start | bytes 786440 | tf_op jit(solution)/shard_map/ppermute | solution.py:195
  35.3 8.5 %collective-permute-start.22 = (bf16[64,2048]{1,0:T(8,128)(2,1)S(1)}, bf16[64,2048]{1,0:T(8,128)(2,1)S(1)}, u32[]{:S(2)}, u32[]{:S(2)}) collective-permute-start(bf16[64,2048]{1,0:T(8,128)(2,1)S(1)} %get-tuple-element.44), channel_id=1, source_target_pairs={{0,16},{4,20},{8,24},{12,28},{16,0},{20,4},{24,8},{28,12},{1,17},{... | collective-permute-start | bytes 786440 | tf_op jit(solution)/shard_map/ppermute | solution.py:195
  43.7 12.1 %collective-permute-start.23 = (bf16[64,2048]{1,0:T(8,128)(2,1)S(1)}, bf16[64,2048]{1,0:T(8,128)(2,1)S(1)}, u32[]{:S(2)}, u32[]{:S(2)}) collective-permute-start(bf16[64,2048]{1,0:T(8,128)(2,1)S(1)} %get-tuple-element.45), channel_id=1, source_target_pairs={{0,20},{4,16},{8,28},{12,24},{16,4},{20,0},{24,12},{28,8},{1,21},{... | collective-permute-start | bytes 786440 | tf_op jit(solution)/shard_map/ppermute | solution.py:195
  55.9 5.3 %collective-permute-done.22.refs_0_ = bf16[64,2048]{1,0:T(8,128)(2,1)S(1)} collective-permute-done((bf16[64,2048]{1,0:T(8,128)(2,1)S(1)}, bf16[64,2048]{1,0:T(8,128)(2,1)S(1)}, u32[]{:S(2)}, u32[]{:S(2)}) %collective-permute-start.22) | collective-permute-done | bytes 262176 | tf_op jit(solution)/shard_map/ppermute | solution.py:195
  61.2 0.5 collective-permute-start.13
  61.7 4.3 %collective-permute-done.23.refs_1_ = bf16[64,2048]{1,0:T(8,128)(2,1)S(1)} collective-permute-done((bf16[64,2048]{1,0:T(8,128)(2,1)S(1)}, bf16[64,2048]{1,0:T(8,128)(2,1)S(1)}, u32[]{:S(2)}, u32[]{:S(2)}) %collective-permute-start.23) | collective-permute-done | bytes 262176 | tf_op jit(solution)/shard_map/ppermute | solution.py:195
  66.5 1.6 collective-permute-done.13.refs_3_
  68.1 0.6 collective-permute-start.15
  68.7 6.5 %collective-permute-done.14.refs_4_ = bf16[64,2048]{1,0:T(8,128)(2,1)S(1)} collective-permute-done((bf16[64,2048]{1,0:T(8,128)(2,1)S(1)}, bf16[64,2048]{1,0:T(8,128)(2,1)S(1)}, u32[]{:S(2)}, u32[]{:S(2)}) %collective-permute-start.14) | collective-permute-done | bytes 262176 | tf_op jit(solution)/shard_map/ppermute | solution.py:195
  75.2 0.5 collective-permute-start.32
  75.7 5.1 %collective-permute-done.15.refs_5_ = bf16[64,2048]{1,0:T(8,128)(2,1)S(1)} collective-permute-done((bf16[64,2048]{1,0:T(8,128)(2,1)S(1)}, bf16[64,2048]{1,0:T(8,128)(2,1)S(1)}, u32[]{:S(2)}, u32[]{:S(2)}) %collective-permute-start.15) | collective-permute-done | bytes 262176 | tf_op jit(solution)/shard_map/ppermute | solution.py:195
  80.8 0.5 collective-permute-start.33
  81.3 5.1 %collective-permute-done.32.refs_2_ = bf16[64,2048]{1,0:T(8,128)(2,1)S(1)} collective-permute-done((bf16[64,2048]{1,0:T(8,128)(2,1)S(1)}, bf16[64,2048]{1,0:T(8,128)(2,1)S(1)}, u32[]{:S(2)}, u32[]{:S(2)}) %collective-permute-start.32) | collective-permute-done | bytes 262176 | tf_op jit(solution)/shard_map/ppermute | solution.py:195
  86.4 0.5 collective-permute-start.24
  86.9 5.1 %collective-permute-done.33.refs_3_ = bf16[64,2048]{1,0:T(8,128)(2,1)S(1)} collective-permute-done((bf16[64,2048]{1,0:T(8,128)(2,1)S(1)}, bf16[64,2048]{1,0:T(8,128)(2,1)S(1)}, u32[]{:S(2)}, u32[]{:S(2)}) %collective-permute-start.33) | collective-permute-done | bytes 262176 | tf_op jit(solution)/shard_map/ppermute | solution.py:195
  92.0 0.5 collective-permute-start.1
  92.6 5.1 %collective-permute-done.24.refs_2_ = bf16[64,2048]{1,0:T(8,128)(2,1)S(1)} collective-permute-done((bf16[64,2048]{1,0:T(8,128)(2,1)S(1)}, bf16[64,2048]{1,0:T(8,128)(2,1)S(1)}, u32[]{:S(2)}, u32[]{:S(2)}) %collective-permute-start.24) | collective-permute-done | bytes 262176 | tf_op jit(solution)/shard_map/ppermute | solution.py:195
  98.2 0.9 slice_bitcast_fusion
  99.1 0.6 collective-permute-start.25
  99.8 1.4 copy-done
  101.2 1.4 copy-done.2
  102.6 1.4 copy-done.4
  104.0 3.6 %shard_map.179 = (bf16[64,2048]{1,0:T(8,128)(2,1)S(1)}, bf16[64,2048]{1,0:T(8,128)(2,1)S(1)}, bf16[64,2048]{1,0:T(8,128)(2,1)S(1)}, bf16[64,2048]{1,0:T(8,128)(2...) custom-call(bf16[64,2048]{1,0:T(8,128)(2,1)S(1)} %collective-permute-done.10.refs_0_, ...), custom_call_target="tpu_custom_call" | custom-call | flops 1811939328 | bytes 12582912 | tf_op jit(solution)/shard_map/pallas_call | solution.py:210
  107.6 4.9 %collective-permute-done.25.refs_3_ = bf16[64,2048]{1,0:T(8,128)(2,1)S(1)} collective-permute-done((bf16[64,2048]{1,0:T(8,128)(2,1)S(1)}, bf16[64,2048]{1,0:T(8,128)(2,1)S(1)}, u32[]{:S(2)}, u32[]{:S(2)}) %collective-permute-start.25) | collective-permute-done | bytes 262176 | tf_op jit(solution)/shard_map/ppermute | solution.py:195
  112.5 0.5 collective-permute-start.20
  113.0 3.3 %shard_map.181 = (bf16[64,2048]{1,0:T(8,128)(2,1)S(1)}, bf16[64,2048]{1,0:T(8,128)(2,1)S(1)}, bf16[64,2048]{1,0:T(8,128)(2,1)S(1)}, bf16[64,2048]{1,0:T(8,128)(2,1)S(1)}) custom-call(bf16[64,2048]{1,0:T(8,128)(2,1)S(1)} %collective-permute-done.30.refs_0_, bf16[64,2048]{1,0:T(8,128)(2,1)S(1)} %collective-permute-done.31.refs_1_, ...), custom_call_target="tpu_custom_call" | custom-call | flops 1207959552 | bytes 11534336 | tf_op jit(solution)/shard_map/pallas_call | solution.py:210
  116.4 3.3 %shard_map.180 = (bf16[64,2048]{1,0:T(8,128)(2,1)S(1)}, bf16[64,2048]{1,0:T(8,128)(2,1)S(1)}, bf16[64,2048]{1,0:T(8,128)(2,1)S(1)}, bf16[64,2048]{1,0:T(8,128)(2,1)S(1)}) custom-call(bf16[64,2048]{1,0:T(8,128)(2,1)S(1)} %collective-permute-done.22.refs_0_, bf16[64,2048]{1,0:T(8,128)(2,1)S(1)} %collective-permute-done.23.refs_1_, ...), custom_call_target="tpu_custom_call" | custom-call | flops 1207959552 | bytes 11534336 | tf_op jit(solution)/shard_map/pallas_call | solution.py:210
  119.7 1.5 collective-permute-start
  121.2 2.2 %collective-permute-start.18 = (bf16[64,2048]{1,0:T(8,128)(2,1)S(1)}, bf16[64,2048]{1,0:T(8,128)(2,1)S(1)}, u32[]{:S(2)}, u32[]{:S(2)}) collective-permute-start(bf16[64,2048]{1,0:T(8,128)(2,1)S(1)} %get-tuple-element.41), channel_id=1, source_target_pairs={{0,2},{1,3},{2,0},{3,1},{4,6},{5,7},{6,4},{7,5},{8,10},{9,11},{10,... | collective-permute-start | bytes 786440 | tf_op jit(solution)/shard_map/ppermute | solution.py:195
  123.4 1.9 collective-permute-start.36
  125.4 5.7 %shard_map.178 = (f32[128,2048]{1,0:T(8,128)S(1)}, bf16[128,2048]{1,0:T(8,128)(2,1)}) custom-call(bf16[128,2048]{1,0:T(8,128)(2,1)S(1)} %get-tuple-element.31.own_ref, bf16[128,2048]{1,0:T(8,128)(2,1)S(1)} %collective-permute-done.1.other_ref, bf16[192,128]{1,0:T(8,128)(2,1)S(1)} %get-tuple-element.32.own_tab, ...), custom_call_target="tpu_custom_call" | custom-call | flops 1409286144 | bytes 15302656 | tf_op jit(solution)/shard_map/pallas_call | solution.py:210
  131.2 2.0 collective-permute-start.28
  133.3 2.4 %collective-permute-done.16 = bf16[64,2048]{1,0:T(8,128)(2,1)S(1)} collective-permute-done((bf16[64,2048]{1,0:T(8,128)(2,1)S(1)}, bf16[64,2048]{1,0:T(8,128)(2,1)S(1)}, u32[]{:S(2)}, u32[]{:S(2)}) %collective-permute-start.16) | collective-permute-done | bytes 262176 | tf_op jit(solution)/shard_map/ppermute | solution.py:195
  135.6 2.5 %collective-permute-start.26 = (bf16[64,2048]{1,0:T(8,128)(2,1)S(1)}, bf16[64,2048]{1,0:T(8,128)(2,1)S(1)}, u32[]{:S(2)}, u32[]{:S(2)}) collective-permute-start(bf16[64,2048]{1,0:T(8,128)(2,1)S(1)} %get-tuple-element.47), channel_id=1, source_target_pairs={{0,2},{1,3},{2,0},{3,1},{4,6},{5,7},{6,4},{7,5},{8,10},{9,11},{10,... | collective-permute-start | bytes 786440 | tf_op jit(solution)/shard_map/ppermute | solution.py:195
  138.2 3.1 %collective-permute-done.36 = bf16[64,2048]{1,0:T(8,128)(2,1)S(1)} collective-permute-done((bf16[64,2048]{1,0:T(8,128)(2,1)S(1)}, bf16[64,2048]{1,0:T(8,128)(2,1)S(1)}, u32[]{:S(2)}, u32[]{:S(2)}) %collective-permute-start.36) | collective-permute-done | bytes 262176 | tf_op jit(solution)/shard_map/ppermute | solution.py:195
  141.3 2.5 %collective-permute-start.9 = (bf16[128,2048]{1,0:T(8,128)(2,1)}, bf16[128,2048]{1,0:T(8,128)(2,1)S(1)}, u32[]{:S(2)}, u32[]{:S(2)}) collective-permute-start(bf16[128,2048]{1,0:T(8,128)(2,1)} %get-tuple-element.34), channel_id=1, source_target_pairs={{0,2},{1,3},{2,0},{3,1},{4,6},{5,7},{6,4},{7,5},{8,10},{9,11},{10,... | collective-permute-start | bytes 1572872 | tf_op jit(solution)/shard_map/ppermute | solution.py:195
  143.8 0.8 add_convert_fusion
  144.5 2.3 %collective-permute-done.34 = bf16[64,2048]{1,0:T(8,128)(2,1)S(1)} collective-permute-done((bf16[64,2048]{1,0:T(8,128)(2,1)S(1)}, bf16[64,2048]{1,0:T(8,128)(2,1)S(1)}, u32[]{:S(2)}, u32[]{:S(2)}) %collective-permute-start.34) | collective-permute-done | bytes 262176 | tf_op jit(solution)/shard_map/ppermute | solution.py:195
  146.9 1.1 collective-permute-start.21
  148.0 0.8 add_convert_fusion.1
  148.7 3.7 %collective-permute-done.28 = bf16[64,2048]{1,0:T(8,128)(2,1)S(1)} collective-permute-done((bf16[64,2048]{1,0:T(8,128)(2,1)S(1)}, bf16[64,2048]{1,0:T(8,128)(2,1)S(1)}, u32[]{:S(2)}, u32[]{:S(2)}) %collective-permute-start.28) | collective-permute-done | bytes 262176 | tf_op jit(solution)/shard_map/ppermute | solution.py:195
  152.5 0.8 add_convert_fusion.2
  153.3 4.8 %collective-permute-done.26 = bf16[64,2048]{1,0:T(8,128)(2,1)S(1)} collective-permute-done((bf16[64,2048]{1,0:T(8,128)(2,1)S(1)}, bf16[64,2048]{1,0:T(8,128)(2,1)S(1)}, u32[]{:S(2)}, u32[]{:S(2)}) %collective-permute-start.26) | collective-permute-done | bytes 262176 | tf_op jit(solution)/shard_map/ppermute | solution.py:195
  158.1 1.8 collective-permute-start.17
  160.0 0.8 add_convert_fusion.3
  160.7 3.7 %collective-permute-start.37 = (bf16[64,2048]{1,0:T(8,128)(2,1)}, bf16[64,2048]{1,0:T(8,128)(2,1)S(1)}, u32[]{:S(2)}, u32[]{:S(2)}) collective-permute-start(bf16[64,2048]{1,0:T(8,128)(2,1)} %add_convert_fusion), channel_id=1, source_target_pairs={{0,28},{4,24},{8,20},{12,16},{16,12},{20,8},{24,4},{28,0},{1,29},{... | collective-permute-start | bytes 786440 | tf_op jit(solution)/shard_map/ppermute | solution.py:195
  165.2 3.5 %collective-permute-start.27 = (bf16[64,2048]{1,0:T(8,128)(2,1)}, bf16[64,2048]{1,0:T(8,128)(2,1)}, u32[]{:S(2)}, u32[]{:S(2)}) collective-permute-start(bf16[64,2048]{1,0:T(8,128)(2,1)} %add_convert_fusion.3), channel_id=1, source_target_pairs={{0,16},{4,20},{8,24},{12,28},{16,0},{20,4},{24,8},{28,12},{1,17},{... | collective-permute-start | bytes 786440 | tf_op jit(solution)/shard_map/ppermute | solution.py:195
  168.7 2.2 %copy-done.6 = bf16[1024,2048]{1,0:T(8,128)(2,1)S(1)} copy-done((bf16[1024,2048]{1,0:T(8,128)(2,1)S(1)}, bf16[1024,2048]{1,0:T(8,128)(2,1)}, u32[]{:S(2)}) %copy-start.6) | copy-done | bytes 4194328
  170.9 9.4 %shard_map.176 = bf16[256,2048]{1,0:T(8,128)(2,1)} custom-call(bf16[256,1024]{1,0:T(8,128)(2,1)S(1)} %copy-done.7, bf16[256,256]{1,0:T(8,128)(2,1)S(1)} %copy-done.11, bf16[256,256]{1,0:T(8,128)(2,1)S(1)} %copy-done.12, bf16[2,128,256]{2,1,0:T(8,128)(2,1)S(1)} %collective-permute-done.rim_ref, f32[16]{0:T(128)S(1)} %copy-done.19, s32[1]{0:T(128)} %bitcast.2.first_ref, ...), custom_call_target="tpu_custom_call" | custom-call | flops 1610612736 | bytes 5767168 | tf_op jit(solution)/shard_map/pallas_call | solution.py:106
  180.3 23.8 %collective-permute-done.29.refs_4_ = bf16[64,2048]{1,0:T(8,128)(2,1)} collective-permute-done((bf16[64,2048]{1,0:T(8,128)(2,1)}, bf16[64,2048]{1,0:T(8,128)(2,1)}, u32[]{:S(2)}, u32[]{:S(2)}) %collective-permute-start.29) | collective-permute-done | bytes 262176 | tf_op jit(solution)/shard_map/ppermute | solution.py:195
  204.1 2.6 %collective-permute-done.27.refs_3_ = bf16[64,2048]{1,0:T(8,128)(2,1)} collective-permute-done((bf16[64,2048]{1,0:T(8,128)(2,1)}, bf16[64,2048]{1,0:T(8,128)(2,1)}, u32[]{:S(2)}, u32[]{:S(2)}) %collective-permute-start.27) | collective-permute-done | bytes 262176 | tf_op jit(solution)/shard_map/ppermute | solution.py:195
  206.8 2.8 %shard_map.182 = bf16[128,2048]{1,0:T(8,128)(2,1)} custom-call(bf16[448,128]{1,0:T(8,128)(2,1)S(1)} %copy-done.14, bf16[448,128]{1,0:T(8,128)(2,1)S(1)} %copy-done.16, f32[128,2048]{1,0:T(8,128)S(1)} %get-tuple-element.33.shared_ref, bf16[128,2048]{1,0:T(8,128)(2,1)S(1)} %collective-permute-done.9.back_ref, f32[1,2048]{1,0:T(1,128)S(1)} %bitcast.36, ...), custom_call_target="tpu_custom_call" | custom-call | flops 469762048 | bytes 4169728 | tf_op jit(solution)/shard_map/pallas_call | solution.py:210
  (75 shorter events, 3.3 us)
Async XLA Ops:
  1.3 1.0 copy-start.20
  2.4 0.7 copy-start.21
  3.1 0.7 copy-start.22
  4.6 95.1 %copy-start.13 = (bf16[448,128]{1,0:T(8,128)(2,1)}, bf16[448,128]{1,0:T(8,128)(2,1)S(1)}, u32[]{:S(2)}) copy-start(bf16[448,128]{1,0:T(8,128)(2,1)S(1)} %get-tuple-element.29.top_ref) | copy-start | bytes 344068
  4.7 95.1 %copy-start.15 = (bf16[448,128]{1,0:T(8,128)(2,1)}, bf16[448,128]{1,0:T(8,128)(2,1)S(1)}, u32[]{:S(2)}) copy-start(bf16[448,128]{1,0:T(8,128)(2,1)S(1)} %get-tuple-element.30.rest_ref) | copy-start | bytes 344068
  4.7 6.5 %collective-permute-start.2 = (bf16[192,128]{1,0:T(8,128)(2,1)S(1)}, bf16[192,128]{1,0:T(8,128)(2,1)S(1)}, u32[]{:S(2)}, u32[]{:S(2)}) collective-permute-start(bf16[192,128]{1,0:T(8,128)(2,1)S(1)} %get-tuple-element.32.own_tab), channel_id=1, source_target_pairs={{0,2},{1,3},{2,0},{3,1},{4,6},{5,7},{6,4},{7,5},{8,10},{9,11},{10,... | collective-permute-start | bytes 147464 | tf_op jit(solution)/shard_map/ppermute | solution.py:195
  7.7 8.3 %collective-permute-start.10 = (bf16[64,2048]{1,0:T(8,128)(2,1)S(1)}, bf16[64,2048]{1,0:T(8,128)(2,1)S(1)}, u32[]{:S(2)}, u32[]{:S(2)}) collective-permute-start(bf16[64,2048]{1,0:T(8,128)(2,1)S(1)} %get-tuple-element.35), channel_id=1, source_target_pairs={{0,4},{4,0},{8,12},{12,8},{16,20},{20,16},{24,28},{28,24},{1,5},{5... | collective-permute-start | bytes 786440 | tf_op jit(solution)/shard_map/ppermute | solution.py:195
  9.2 9.2 %collective-permute-start.11 = (bf16[64,2048]{1,0:T(8,128)(2,1)S(1)}, bf16[64,2048]{1,0:T(8,128)(2,1)S(1)}, u32[]{:S(2)}, u32[]{:S(2)}) collective-permute-start(bf16[64,2048]{1,0:T(8,128)(2,1)S(1)} %get-tuple-element.36), channel_id=1, source_target_pairs={{0,8},{4,12},{8,0},{12,4},{16,24},{20,28},{24,16},{28,20},{1,9},{5... | collective-permute-start | bytes 786440 | tf_op jit(solution)/shard_map/ppermute | solution.py:195
  10.8 11.8 %collective-permute-start.12 = (bf16[64,2048]{1,0:T(8,128)(2,1)S(1)}, bf16[64,2048]{1,0:T(8,128)(2,1)S(1)}, u32[]{:S(2)}, u32[]{:S(2)}) collective-permute-start(bf16[64,2048]{1,0:T(8,128)(2,1)S(1)} %get-tuple-element.37), channel_id=1, source_target_pairs={{0,12},{4,8},{8,4},{12,0},{16,28},{20,24},{24,20},{28,16},{1,13},{... | collective-permute-start | bytes 786440 | tf_op jit(solution)/shard_map/ppermute | solution.py:195
  11.2 86.5 %collective-permute-start.6 = (bf16[2,192,2048]{2,1,0:T(8,128)(2,1)}, bf16[2,192,2048]{2,1,0:T(8,128)(2,1)S(1)}, u32[]{:S(2)}, u32[]{:S(2)}) collective-permute-start(bf16[2,192,2048]{2,1,0:T(8,128)(2,1)} %bitcast.25), channel_id=1, source_target_pairs={{0,1},{1,0},{2,3},{3,2},{4,5},{5,4},{6,7},{7,6},{8,9},{9,8},{10,11... | collective-permute-start | bytes 4718600 | tf_op jit(solution)/shard_map/ppermute | solution.py:195
  11.2 87.0 %collective-permute-start.7 = (bf16[2,192,2048]{2,1,0:T(8,128)(2,1)}, bf16[2,192,2048]{2,1,0:T(8,128)(2,1)S(1)}, u32[]{:S(2)}, u32[]{:S(2)}) collective-permute-start(bf16[2,192,2048]{2,1,0:T(8,128)(2,1)} %bitcast.30), channel_id=1, source_target_pairs={{0,1},{1,0},{2,3},{3,2},{4,5},{5,4},{6,7},{7,6},{8,9},{9,8},{10,11... | collective-permute-start | bytes 4718600 | tf_op jit(solution)/shard_map/ppermute | solution.py:195
  16.0 83.1 %collective-permute-start.8 = (bf16[2,192,2048]{2,1,0:T(8,128)(2,1)}, bf16[2,192,2048]{2,1,0:T(8,128)(2,1)S(1)}, u32[]{:S(2)}, u32[]{:S(2)}) collective-permute-start(bf16[2,192,2048]{2,1,0:T(8,128)(2,1)} %refs_8_.3), channel_id=1, source_target_pairs={{0,1},{1,0},{2,3},{3,2},{4,5},{5,4},{6,7},{7,6},{8,9},{9,8},{10,11... | collective-permute-start | bytes 4718600 | tf_op jit(solution)/shard_map/ppermute | solution.py:195
  18.4 16.9 %collective-permute-start.30 = (bf16[64,2048]{1,0:T(8,128)(2,1)S(1)}, bf16[64,2048]{1,0:T(8,128)(2,1)S(1)}, u32[]{:S(2)}, u32[]{:S(2)}) collective-permute-start(bf16[64,2048]{1,0:T(8,128)(2,1)S(1)} %get-tuple-element.50), channel_id=1, source_target_pairs={{0,24},{4,28},{8,16},{12,20},{16,8},{20,12},{24,0},{28,4},{1,25},{... | collective-permute-start | bytes 786440 | tf_op jit(solution)/shard_map/ppermute | solution.py:195
  22.6 21.1 %collective-permute-start.31 = (bf16[64,2048]{1,0:T(8,128)(2,1)S(1)}, bf16[64,2048]{1,0:T(8,128)(2,1)S(1)}, u32[]{:S(2)}, u32[]{:S(2)}) collective-permute-start(bf16[64,2048]{1,0:T(8,128)(2,1)S(1)} %get-tuple-element.51), channel_id=1, source_target_pairs={{0,28},{4,24},{8,20},{12,16},{16,12},{20,8},{24,4},{28,0},{1,29},{... | collective-permute-start | bytes 786440 | tf_op jit(solution)/shard_map/ppermute | solution.py:195
  35.3 25.9 %collective-permute-start.22 = (bf16[64,2048]{1,0:T(8,128)(2,1)S(1)}, bf16[64,2048]{1,0:T(8,128)(2,1)S(1)}, u32[]{:S(2)}, u32[]{:S(2)}) collective-permute-start(bf16[64,2048]{1,0:T(8,128)(2,1)S(1)} %get-tuple-element.44), channel_id=1, source_target_pairs={{0,16},{4,20},{8,24},{12,28},{16,0},{20,4},{24,8},{28,12},{1,17},{... | collective-permute-start | bytes 786440 | tf_op jit(solution)/shard_map/ppermute | solution.py:195
  43.7 22.3 %collective-permute-start.23 = (bf16[64,2048]{1,0:T(8,128)(2,1)S(1)}, bf16[64,2048]{1,0:T(8,128)(2,1)S(1)}, u32[]{:S(2)}, u32[]{:S(2)}) collective-permute-start(bf16[64,2048]{1,0:T(8,128)(2,1)S(1)} %get-tuple-element.45), channel_id=1, source_target_pairs={{0,20},{4,16},{8,28},{12,24},{16,4},{20,0},{24,12},{28,8},{1,21},{... | collective-permute-start | bytes 786440 | tf_op jit(solution)/shard_map/ppermute | solution.py:195
  61.2 6.9 %collective-permute-start.13 = (bf16[64,2048]{1,0:T(8,128)(2,1)S(1)}, bf16[64,2048]{1,0:T(8,128)(2,1)S(1)}, u32[]{:S(2)}, u32[]{:S(2)}) collective-permute-start(bf16[64,2048]{1,0:T(8,128)(2,1)S(1)} %collective-permute-done.10.refs_0_), channel_id=1, source_target_pairs={{0,2},{1,3},{2,0},{3,1},{4,6},{5,7},{6,4},{7,5},{8,10},{9,11},{10,... | collective-permute-start | bytes 786440 | tf_op jit(solution)/shard_map/ppermute | solution.py:195
  66.0 9.2 %collective-permute-start.14 = (bf16[64,2048]{1,0:T(8,128)(2,1)S(1)}, bf16[64,2048]{1,0:T(8,128)(2,1)S(1)}, u32[]{:S(2)}, u32[]{:S(2)}) collective-permute-start(bf16[64,2048]{1,0:T(8,128)(2,1)S(1)} %collective-permute-done.11.refs_1_), channel_id=1, source_target_pairs={{0,2},{1,3},{2,0},{3,1},{4,6},{5,7},{6,4},{7,5},{8,10},{9,11},{10,... | collective-permute-start | bytes 786440 | tf_op jit(solution)/shard_map/ppermute | solution.py:195
  68.1 12.7 %collective-permute-start.15 = (bf16[64,2048]{1,0:T(8,128)(2,1)S(1)}, bf16[64,2048]{1,0:T(8,128)(2,1)S(1)}, u32[]{:S(2)}, u32[]{:S(2)}) collective-permute-start(bf16[64,2048]{1,0:T(8,128)(2,1)S(1)} %collective-permute-done.12.refs_2_), channel_id=1, source_target_pairs={{0,2},{1,3},{2,0},{3,1},{4,6},{5,7},{6,4},{7,5},{8,10},{9,11},{10,... | collective-permute-start | bytes 786440 | tf_op jit(solution)/shard_map/ppermute | solution.py:195
  75.2 11.2 %collective-permute-start.32 = (bf16[64,2048]{1,0:T(8,128)(2,1)S(1)}, bf16[64,2048]{1,0:T(8,128)(2,1)S(1)}, u32[]{:S(2)}, u32[]{:S(2)}) collective-permute-start(bf16[64,2048]{1,0:T(8,128)(2,1)S(1)} %collective-permute-done.30.refs_0_), channel_id=1, source_target_pairs={{0,2},{1,3},{2,0},{3,1},{4,6},{5,7},{6,4},{7,5},{8,10},{9,11},{10,... | collective-permute-start | bytes 786440 | tf_op jit(solution)/shard_map/ppermute | solution.py:195
  80.8 11.2 %collective-permute-start.33 = (bf16[64,2048]{1,0:T(8,128)(2,1)S(1)}, bf16[64,2048]{1,0:T(8,128)(2,1)S(1)}, u32[]{:S(2)}, u32[]{:S(2)}) collective-permute-start(bf16[64,2048]{1,0:T(8,128)(2,1)S(1)} %collective-permute-done.31.refs_1_), channel_id=1, source_target_pairs={{0,2},{1,3},{2,0},{3,1},{4,6},{5,7},{6,4},{7,5},{8,10},{9,11},{10,... | collective-permute-start | bytes 786440 | tf_op jit(solution)/shard_map/ppermute | solution.py:195
  86.4 11.2 %collective-permute-start.24 = (bf16[64,2048]{1,0:T(8,128)(2,1)S(1)}, bf16[64,2048]{1,0:T(8,128)(2,1)S(1)}, u32[]{:S(2)}, u32[]{:S(2)}) collective-permute-start(bf16[64,2048]{1,0:T(8,128)(2,1)S(1)} %collective-permute-done.22.refs_0_), channel_id=1, source_target_pairs={{0,2},{1,3},{2,0},{3,1},{4,6},{5,7},{6,4},{7,5},{8,10},{9,11},{10,... | collective-permute-start | bytes 786440 | tf_op jit(solution)/shard_map/ppermute | solution.py:195
  92.0 27.6 %collective-permute-start.1 = (bf16[128,2048]{1,0:T(8,128)(2,1)S(1)}, bf16[128,2048]{1,0:T(8,128)(2,1)S(1)}, u32[]{:S(2)}, u32[]{:S(2)}) collective-permute-start(bf16[128,2048]{1,0:T(8,128)(2,1)S(1)} %get-tuple-element.31.own_ref), channel_id=1, source_target_pairs={{0,2},{1,3},{2,0},{3,1},{4,6},{5,7},{6,4},{7,5},{8,10},{9,11},{10,... | collective-permute-start | bytes 1572872 | tf_op jit(solution)/shard_map/ppermute | solution.py:195
  97.6 23.5 %collective-permute-start.3 = (bf16[2048,128]{1,0:T(8,128)(2,1)}, bf16[2048,128]{1,0:T(8,128)(2,1)S(1)}, u32[]{:S(2)}, u32[]{:S(2)}) collective-permute-start(bf16[2048,128]{1,0:T(8,128)(2,1)} %refs_0_.1), channel_id=1, source_target_pairs={{0,1},{1,0},{2,3},{3,2},{4,5},{5,4},{6,7},{7,6},{8,9},{9,8},{10,11... | collective-permute-start | bytes 1572872 | tf_op jit(solution)/shard_map/ppermute | solution.py:195
  97.7 25.7 %collective-permute-start.4 = (bf16[2048,128]{1,0:T(8,128)(2,1)}, bf16[2048,128]{1,0:T(8,128)(2,1)S(1)}, u32[]{:S(2)}, u32[]{:S(2)}) collective-permute-start(bf16[2048,128]{1,0:T(8,128)(2,1)} %refs_2_.1), channel_id=1, source_target_pairs={{0,1},{1,0},{2,3},{3,2},{4,5},{5,4},{6,7},{7,6},{8,9},{9,8},{10,11... | collective-permute-start | bytes 1572872 | tf_op jit(solution)/shard_map/ppermute | solution.py:195
  98.2 25.2 %collective-permute-start.5 = (bf16[128,2048]{1,0:T(8,128)(2,1)}, bf16[128,2048]{1,0:T(8,128)(2,1)S(1)}, u32[]{:S(2)}, u32[]{:S(2)}) collective-permute-start(bf16[128,2048]{1,0:T(8,128)(2,1)} %refs_4_.1), channel_id=1, source_target_pairs={{0,1},{1,0},{2,3},{3,2},{4,5},{5,4},{6,7},{7,6},{8,9},{9,8},{10,11... | collective-permute-start | bytes 1572872 | tf_op jit(solution)/shard_map/ppermute | solution.py:195
  99.1 13.4 %collective-permute-start.25 = (bf16[64,2048]{1,0:T(8,128)(2,1)S(1)}, bf16[64,2048]{1,0:T(8,128)(2,1)S(1)}, u32[]{:S(2)}, u32[]{:S(2)}) collective-permute-start(bf16[64,2048]{1,0:T(8,128)(2,1)S(1)} %collective-permute-done.23.refs_1_), channel_id=1, source_target_pairs={{0,2},{1,3},{2,0},{3,1},{4,6},{5,7},{6,4},{7,5},{8,10},{9,11},{10,... | collective-permute-start | bytes 786440 | tf_op jit(solution)/shard_map/ppermute | solution.py:195
  99.8 1.4 copy-start
  101.2 1.4 copy-start.2
  102.6 1.4 copy-start.4
  112.5 18.6 %collective-permute-start.20 = (bf16[64,2048]{1,0:T(8,128)(2,1)S(1)}, bf16[64,2048]{1,0:T(8,128)(2,1)S(1)}, u32[]{:S(2)}, u32[]{:S(2)}) collective-permute-start(bf16[64,2048]{1,0:T(8,128)(2,1)S(1)} %get-tuple-element.43), channel_id=1, source_target_pairs={{0,2},{1,3},{2,0},{3,1},{4,6},{5,7},{6,4},{7,5},{8,10},{9,11},{10,... | collective-permute-start | bytes 786440 | tf_op jit(solution)/shard_map/ppermute | solution.py:195
  116.3 9.1 %copy-start.1 = (bf16[2,2048,192]{1,2,0:T(8,128)(2,1)S(1)}, bf16[2,2048,192]{1,2,0:T(8,128)(2,1)}, u32[]{:S(2)}) copy-start(bf16[2,2048,192]{1,2,0:T(8,128)(2,1)} %param.27) | copy-start | bytes 4718596
  116.3 9.0 %copy-start.3 = (bf16[2,2048,192]{1,2,0:T(8,128)(2,1)S(1)}, bf16[2,2048,192]{1,2,0:T(8,128)(2,1)}, u32[]{:S(2)}) copy-start(bf16[2,2048,192]{1,2,0:T(8,128)(2,1)} %param.28) | copy-start | bytes 4718596
  116.3 9.0 %copy-start.5 = (bf16[2,192,2048]{2,1,0:T(8,128)(2,1)S(1)}, bf16[2,192,2048]{2,1,0:T(8,128)(2,1)}, u32[]{:S(2)}) copy-start(bf16[2,192,2048]{2,1,0:T(8,128)(2,1)} %refs_8_.3) | copy-start | bytes 4718596
  116.3 9.0 %copy-start.8 = (bf16[2048,128]{1,0:T(8,128)(2,1)S(1)}, bf16[2048,128]{1,0:T(8,128)(2,1)}, u32[]{:S(2)}) copy-start(bf16[2048,128]{1,0:T(8,128)(2,1)} %refs_0_.1) | copy-start | bytes 1572868
  116.3 9.0 %copy-start.9 = (bf16[2048,128]{1,0:T(8,128)(2,1)S(1)}, bf16[2048,128]{1,0:T(8,128)(2,1)}, u32[]{:S(2)}) copy-start(bf16[2048,128]{1,0:T(8,128)(2,1)} %refs_2_.1) | copy-start | bytes 1572868
  116.4 9.0 %copy-start.10 = (bf16[128,2048]{1,0:T(8,128)(2,1)S(1)}, bf16[128,2048]{1,0:T(8,128)(2,1)}, u32[]{:S(2)}) copy-start(bf16[128,2048]{1,0:T(8,128)(2,1)} %refs_4_.1) | copy-start | bytes 1572868
  119.7 41.1 %collective-permute-start = (bf16[2,128,256]{2,1,0:T(8,128)(2,1)S(1)}, bf16[2,128,256]{2,1,0:T(8,128)(2,1)S(1)}, u32[]{:S(2)}, u32[]{:S(2)}) collective-permute-start(bf16[2,128,256]{2,1,0:T(8,128)(2,1)S(1)} %pad_maximum_fusion), channel_id=1, source_target_pairs={{0,1},{1,2},{2,3},{3,4},{4,5},{5,6},{6,7},{7,8},{8,9},{9,10},{10,1... | collective-permute-start | bytes 393224 | tf_op jit(solution)/shard_map/ppermute | solution.py:26
  121.2 10.1 %collective-permute-start.18 = (bf16[64,2048]{1,0:T(8,128)(2,1)S(1)}, bf16[64,2048]{1,0:T(8,128)(2,1)S(1)}, u32[]{:S(2)}, u32[]{:S(2)}) collective-permute-start(bf16[64,2048]{1,0:T(8,128)(2,1)S(1)} %get-tuple-element.41), channel_id=1, source_target_pairs={{0,2},{1,3},{2,0},{3,1},{4,6},{5,7},{6,4},{7,5},{8,10},{9,11},{10,... | collective-permute-start | bytes 786440 | tf_op jit(solution)/shard_map/ppermute | solution.py:195
  123.3 12.3 %collective-permute-start.16 = (bf16[64,2048]{1,0:T(8,128)(2,1)S(1)}, bf16[64,2048]{1,0:T(8,128)(2,1)S(1)}, u32[]{:S(2)}, u32[]{:S(2)}) collective-permute-start(bf16[64,2048]{1,0:T(8,128)(2,1)S(1)} %get-tuple-element.39), channel_id=1, source_target_pairs={{0,2},{1,3},{2,0},{3,1},{4,6},{5,7},{6,4},{7,5},{8,10},{9,11},{10,... | collective-permute-start | bytes 786440 | tf_op jit(solution)/shard_map/ppermute | solution.py:195
  123.4 17.8 %collective-permute-start.36 = (bf16[64,2048]{1,0:T(8,128)(2,1)S(1)}, bf16[64,2048]{1,0:T(8,128)(2,1)S(1)}, u32[]{:S(2)}, u32[]{:S(2)}) collective-permute-start(bf16[64,2048]{1,0:T(8,128)(2,1)S(1)} %get-tuple-element.55), channel_id=1, source_target_pairs={{0,2},{1,3},{2,0},{3,1},{4,6},{5,7},{6,4},{7,5},{8,10},{9,11},{10,... | collective-permute-start | bytes 786440 | tf_op jit(solution)/shard_map/ppermute | solution.py:195
  131.0 15.8 %collective-permute-start.34 = (bf16[64,2048]{1,0:T(8,128)(2,1)S(1)}, bf16[64,2048]{1,0:T(8,128)(2,1)S(1)}, u32[]{:S(2)}, u32[]{:S(2)}) collective-permute-start(bf16[64,2048]{1,0:T(8,128)(2,1)S(1)} %get-tuple-element.53), channel_id=1, source_target_pairs={{0,2},{1,3},{2,0},{3,1},{4,6},{5,7},{6,4},{7,5},{8,10},{9,11},{10,... | collective-permute-start | bytes 786440 | tf_op jit(solution)/shard_map/ppermute | solution.py:195
  131.2 21.3 %collective-permute-start.28 = (bf16[64,2048]{1,0:T(8,128)(2,1)S(1)}, bf16[64,2048]{1,0:T(8,128)(2,1)S(1)}, u32[]{:S(2)}, u32[]{:S(2)}) collective-permute-start(bf16[64,2048]{1,0:T(8,128)(2,1)S(1)} %get-tuple-element.49), channel_id=1, source_target_pairs={{0,2},{1,3},{2,0},{3,1},{4,6},{5,7},{6,4},{7,5},{8,10},{9,11},{10,... | collective-permute-start | bytes 786440 | tf_op jit(solution)/shard_map/ppermute | solution.py:195
  135.6 22.5 %collective-permute-start.26 = (bf16[64,2048]{1,0:T(8,128)(2,1)S(1)}, bf16[64,2048]{1,0:T(8,128)(2,1)S(1)}, u32[]{:S(2)}, u32[]{:S(2)}) collective-permute-start(bf16[64,2048]{1,0:T(8,128)(2,1)S(1)} %get-tuple-element.47), channel_id=1, source_target_pairs={{0,2},{1,3},{2,0},{3,1},{4,6},{5,7},{6,4},{7,5},{8,10},{9,11},{10,... | collective-permute-start | bytes 786440 | tf_op jit(solution)/shard_map/ppermute | solution.py:195
  141.3 65.5 %collective-permute-start.9 = (bf16[128,2048]{1,0:T(8,128)(2,1)}, bf16[128,2048]{1,0:T(8,128)(2,1)S(1)}, u32[]{:S(2)}, u32[]{:S(2)}) collective-permute-start(bf16[128,2048]{1,0:T(8,128)(2,1)} %get-tuple-element.34), channel_id=1, source_target_pairs={{0,2},{1,3},{2,0},{3,1},{4,6},{5,7},{6,4},{7,5},{8,10},{9,11},{10,... | collective-permute-start | bytes 1572872 | tf_op jit(solution)/shard_map/ppermute | solution.py:195
  143.7 25.0 %copy-start.7 = (bf16[256,1024]{1,0:T(8,128)(2,1)S(1)}, bf16[256,1024]{1,0:T(8,128)(2,1)}, u32[]{:S(2)}) copy-start(bf16[256,1024]{1,0:T(8,128)(2,1)} %q_ref.1) | copy-start | bytes 1572868
  143.7 25.0 %copy-start.11 = (bf16[256,256]{1,0:T(8,128)(2,1)S(1)}, bf16[256,256]{1,0:T(8,128)(2,1)}, u32[]{:S(2)}) copy-start(bf16[256,256]{1,0:T(8,128)(2,1)} %k_ref.1) | copy-start | bytes 393220
  143.7 25.0 %copy-start.12 = (bf16[256,256]{1,0:T(8,128)(2,1)S(1)}, bf16[256,256]{1,0:T(8,128)(2,1)}, u32[]{:S(2)}) copy-start(bf16[256,256]{1,0:T(8,128)(2,1)} %v_ref.1) | copy-start | bytes 393220
  143.7 25.0 %copy-start.17 = (f32[2048]{0:T(1024)S(1)}, f32[2048]{0:T(1024)}, u32[]{:S(2)}) copy-start(f32[2048]{0:T(1024)} %param.22) | copy-start | bytes 24580
  143.7 25.0 %copy-start.19 = (f32[16]{0:T(128)S(1)}, f32[16]{0:T(128)}, u32[]{:S(2)}) copy-start(f32[16]{0:T(128)} %sink_ref.1) | copy-start | bytes 196
  146.9 17.6 %collective-permute-start.21 = (bf16[64,2048]{1,0:T(8,128)(2,1)S(1)}, bf16[64,2048]{1,0:T(8,128)(2,1)S(1)}, u32[]{:S(2)}, u32[]{:S(2)}) collective-permute-start(bf16[64,2048]{1,0:T(8,128)(2,1)S(1)} %add_convert_fusion.4), channel_id=1, source_target_pairs={{0,12},{4,8},{8,4},{12,0},{16,28},{20,24},{24,20},{28,16},{1,13},{... | collective-permute-start | bytes 786440 | tf_op jit(solution)/shard_map/ppermute | solution.py:195
  152.5 12.4 %collective-permute-start.19 = (bf16[64,2048]{1,0:T(8,128)(2,1)S(1)}, bf16[64,2048]{1,0:T(8,128)(2,1)S(1)}, u32[]{:S(2)}, u32[]{:S(2)}) collective-permute-start(bf16[64,2048]{1,0:T(8,128)(2,1)S(1)} %add_convert_fusion.5), channel_id=1, source_target_pairs={{0,8},{4,12},{8,0},{12,4},{16,24},{20,28},{24,16},{28,20},{1,9},{5... | collective-permute-start | bytes 786440 | tf_op jit(solution)/shard_map/ppermute | solution.py:195
  158.1 7.1 %collective-permute-start.17 = (bf16[64,2048]{1,0:T(8,128)(2,1)S(1)}, bf16[64,2048]{1,0:T(8,128)(2,1)S(1)}, u32[]{:S(2)}, u32[]{:S(2)}) collective-permute-start(bf16[64,2048]{1,0:T(8,128)(2,1)S(1)} %add_convert_fusion.6), channel_id=1, source_target_pairs={{0,4},{4,0},{8,12},{12,8},{16,20},{20,16},{24,28},{28,24},{1,5},{5... | collective-permute-start | bytes 786440 | tf_op jit(solution)/shard_map/ppermute | solution.py:195
  160.7 19.6 %collective-permute-start.37 = (bf16[64,2048]{1,0:T(8,128)(2,1)}, bf16[64,2048]{1,0:T(8,128)(2,1)S(1)}, u32[]{:S(2)}, u32[]{:S(2)}) collective-permute-start(bf16[64,2048]{1,0:T(8,128)(2,1)} %add_convert_fusion), channel_id=1, source_target_pairs={{0,28},{4,24},{8,20},{12,16},{16,12},{20,8},{24,4},{28,0},{1,29},{... | collective-permute-start | bytes 786440 | tf_op jit(solution)/shard_map/ppermute | solution.py:195
  164.4 15.9 %collective-permute-start.35 = (bf16[64,2048]{1,0:T(8,128)(2,1)}, bf16[64,2048]{1,0:T(8,128)(2,1)}, u32[]{:S(2)}, u32[]{:S(2)}) collective-permute-start(bf16[64,2048]{1,0:T(8,128)(2,1)} %add_convert_fusion.1), channel_id=1, source_target_pairs={{0,24},{4,28},{8,16},{12,20},{16,8},{20,12},{24,0},{28,4},{1,25},{... | collective-permute-start | bytes 786440 | tf_op jit(solution)/shard_map/ppermute | solution.py:195
  164.9 39.3 %collective-permute-start.29 = (bf16[64,2048]{1,0:T(8,128)(2,1)}, bf16[64,2048]{1,0:T(8,128)(2,1)}, u32[]{:S(2)}, u32[]{:S(2)}) collective-permute-start(bf16[64,2048]{1,0:T(8,128)(2,1)} %add_convert_fusion.2), channel_id=1, source_target_pairs={{0,20},{4,16},{8,28},{12,24},{16,4},{20,0},{24,12},{28,8},{1,21},{... | collective-permute-start | bytes 786440 | tf_op jit(solution)/shard_map/ppermute | solution.py:195
  165.2 41.5 %collective-permute-start.27 = (bf16[64,2048]{1,0:T(8,128)(2,1)}, bf16[64,2048]{1,0:T(8,128)(2,1)}, u32[]{:S(2)}, u32[]{:S(2)}) collective-permute-start(bf16[64,2048]{1,0:T(8,128)(2,1)} %add_convert_fusion.3), channel_id=1, source_target_pairs={{0,16},{4,20},{8,24},{12,28},{16,0},{20,4},{24,8},{28,12},{1,17},{... | collective-permute-start | bytes 786440 | tf_op jit(solution)/shard_map/ppermute | solution.py:195
  168.7 2.2 %copy-start.6 = (bf16[1024,2048]{1,0:T(8,128)(2,1)S(1)}, bf16[1024,2048]{1,0:T(8,128)(2,1)}, u32[]{:S(2)}) copy-start(bf16[1024,2048]{1,0:T(8,128)(2,1)} %weight_ref.1) | copy-start | bytes 12582916
  170.9 35.9 %copy-start.14 = (bf16[448,128]{1,0:T(8,128)(2,1)S(1)}, bf16[448,128]{1,0:T(8,128)(2,1)}, u32[]{:S(2)}) copy-start(bf16[448,128]{1,0:T(8,128)(2,1)} %copy-done.13) | copy-start | bytes 344068
  170.9 35.9 %copy-start.16 = (bf16[448,128]{1,0:T(8,128)(2,1)S(1)}, bf16[448,128]{1,0:T(8,128)(2,1)}, u32[]{:S(2)}) copy-start(bf16[448,128]{1,0:T(8,128)(2,1)} %copy-done.15) | copy-start | bytes 344068
  170.9 35.9 %copy-start.18 = (f32[2048]{0:T(1024)S(1)}, f32[2048]{0:T(1024)}, u32[]{:S(2)}) copy-start(f32[2048]{0:T(1024)} %param.33) | copy-start | bytes 24580

commit v2 on v1

--- a/solution.py
+++ b/solution.py
@@ -215,7 +215,7 @@
     )(*operands)
 
 
-def prepare_kernel(cap, in_ref, gain_ref, rel_ref, weight_ref, normed_ref, top_ref, rest_ref, near_ref, *pieces):
+def prepare_kernel(cap, in_ref, gain_ref, rel_ref, weight_ref, normed_ref, slot_ref, near_ref, *pieces):
     rows = in_ref[...].astype(jnp.float32)
     mean_sq = jnp.mean(rows * rows, axis=-1, keepdims=True)
     normed = (rows * lax.rsqrt(mean_sq + EPS) * gain_ref[...]).astype(jnp.bfloat16)
@@ -237,13 +237,14 @@
     )
     slot_row = lax.broadcasted_iota(jnp.int32, (slots, tokens), 0)
     chosen = jnp.zeros((slots, tokens), jnp.float32)
-    share = jnp.zeros((slots, tokens), jnp.float32)
+    share = jnp.zeros((piece_rows, tokens), jnp.float32)
     for k, hit in enumerate(named):
         position = jnp.sum(jnp.where(hit, prior, 0.0), axis=0, keepdims=True)
         slot = rel_ref[k : k + 1, :] * cap + position.astype(jnp.int32)
+        slot_ref[k : k + 1, :] = slot
         here = slot == slot_row
         chosen = chosen + jnp.where(here, 1.0, 0.0)
-        share = share + jnp.where(here, weight_ref[k : k + 1, :], 0.0)
+        share = share + jnp.where(here[:piece_rows], weight_ref[k : k + 1, :], 0.0)
     chosen = chosen.astype(jnp.bfloat16)
     for p, piece in enumerate(pieces, 1):
         piece[...] = jnp.dot(
@@ -253,9 +254,7 @@
         ).astype(jnp.bfloat16)
     top = share.astype(jnp.bfloat16)
     rest = (share - top.astype(jnp.float32)).astype(jnp.bfloat16)
-    top_ref[...] = top[piece_rows:]
-    rest_ref[...] = rest[piece_rows:]
-    near_ref[...] = jnp.concatenate([t[:piece_rows] for t in (chosen, top, rest)], axis=0)
+    near_ref[...] = jnp.concatenate([chosen[:piece_rows], top, rest], axis=0)
 
 
 def routed(rows, j, gate_a, gate_b, up_a, up_b, down_a, down_b):
@@ -312,13 +311,23 @@
         out_ref[...] = (half + share).astype(out_ref.dtype)
 
 
-def combine_kernel(top_ref, rest_ref, shared_ref, back_ref, gain_ref, *refs):
+def combine_kernel(slot_ref, weight_ref, shared_ref, back_ref, gain_ref, *refs):
     pieces, out_ref = refs[:-1], refs[-1]
+    top_count, tokens = slot_ref.shape
+    piece_rows = pieces[0].shape[0]
+    far_rows = len(pieces) * piece_rows
+    slot_row = lax.broadcasted_iota(jnp.int32, (far_rows, tokens), 0) + piece_rows
+    share = jnp.zeros((far_rows, tokens), jnp.float32)
+    for k in range(top_count):
+        here = slot_ref[k : k + 1, :] == slot_row
+        share = share + jnp.where(here, weight_ref[k : k + 1, :], 0.0)
+    top = share.astype(jnp.bfloat16)
+    rest = (share - top.astype(jnp.float32)).astype(jnp.bfloat16)
     rows = jnp.concatenate([piece[...] for piece in pieces], axis=0)
     total = shared_ref[...] + back_ref[...].astype(jnp.float32)
-    for table in (top_ref, rest_ref):
+    for table in (top, rest):
         total = total + lax.dot_general(
-            table[...], rows, (((0,), (0,)), ((), ())), preferred_element_type=jnp.float32
+            table, rows, (((0,), (0,)), ((), ())), preferred_element_type=jnp.float32
         )
     mean_sq = jnp.mean(total * total, axis=-1, keepdims=True)
     out_ref[...] = (total * lax.rsqrt(mean_sq + EPS) * gain_ref[...]).astype(jnp.bfloat16)
@@ -363,11 +372,11 @@
     ids = expert_ids.T
     relative = ((ids // local_experts) ^ own) * local_experts + ids % local_experts
     far_rows = (ep_size - 1) * piece_rows
-    table = jax.ShapeDtypeStruct((far_rows, tokens), jnp.bfloat16)
+    slot_table_shape = jax.ShapeDtypeStruct((top_count, tokens), jnp.int32)
     near_table = jax.ShapeDtypeStruct((3 * piece_rows, tokens), jnp.bfloat16)
-    normed, top, rest, near_tab, *pieces = run_kernel(
+    normed, slots, near_tab, *pieces = run_kernel(
         functools.partial(prepare_kernel, cap),
-        (array(tokens), table, table, near_table) + (array(piece_rows),) * (ep_size - 1),
+        (array(tokens), slot_table_shape, near_table) + (array(piece_rows),) * (ep_size - 1),
         2 * ep_size * piece_rows * tokens * width,
         moe_in,
         pre_gain[None],
@@ -410,8 +419,8 @@
         combine_kernel,
         (array(tokens),),
         2 * 2 * far_rows * tokens * width,
-        top,
-        rest,
+        slots,
+        routed_expert_weight.T,
         local_own,
         local_back,
         moe_gain[None],
@@ -424,7 +433,7 @@
 
 
 def is_near(ep_size, tp_size):
-    return ep_size <= NEAR_LIMIT and ep_size & (ep_size - 1) == 0 and tp_size == 4
+    return ep_size == NEAR_LIMIT and tp_size == 4
 
 
 def body(*args):

time: 211 us -> 211 us (level)
    unnamed x46 -> x40, local copies, waits for them, and re-layouts: 8.89 us -> 8.88 us
where the time goes in v2:
time: 211 us; the launch traced here: 210 us
  waiting for transfers between devices  93.4 us (44%)
  starting transfers between devices  72.7 us (34%)
  Pallas kernels  28.9 us (14%)
  local copies, waits for them, and re-layouts  9.76 us (5%)
  other arithmetic  4 us (2%)
    ppermute x37, waiting for transfers between devices, swap(): return lax.ppermute(block, axis, route)  93.3 us
    ppermute x37, starting transfers between devices, swap(): return lax.ppermute(block, axis, route)  71.2 us
    pallas_call x6, Pallas kernels, run_kernel(): pl.pallas_call(kernel, out_shape=outs, compiler_params=pltpu.CompilerPara...  19.5 us
    pallas_call x1, Pallas kernels, attention(): pl.pallas_call(attention_kernel, out_shape=jax.ShapeDtypeStruct((rows, wi...  9.42 us
    unnamed x40, local copies, waits for them, and re-layouts  8.88 us
  transfers between devices with their start and end apart: 38, of which 20 were waited for; matrix products, arithmetic and copies ran while one was open for 2% of the time, Pallas kernels for 12%

profile of v2, /device:TPU:0, one launch (start us, length us, event | category | flops | bytes accessed | tf_op | source)
XLA Modules:
  0.0 209.6 jit_solution(6812321973373538551)
XLA Ops:
  0.6 0.7 fusion.rel_ref
  1.3 0.7 copy-done.15
  2.0 1.0 copy-done.18
  3.1 0.7 copy-done.19
  3.8 0.9 shard_map.177
  4.6 3.0 %collective-permute-start.2 = (bf16[192,128]{1,0:T(8,128)(2,1)S(1)}, bf16[192,128]{1,0:T(8,128)(2,1)S(1)}, u32[]{:S(2)}, u32[]{:S(2)}) collective-permute-start(bf16[192,128]{1,0:T(8,128)(2,1)S(1)} %get-tuple-element.30.own_tab), channel_id=1, source_target_pairs={{0,2},{1,3},{2,0},{3,1},{4,6},{5,7},{6,4},{7,5},{8,10},{9,11},{10,... | collective-permute-start | bytes 147464 | tf_op jit(solution)/shard_map/ppermute | solution.py:195
  7.6 1.5 collective-permute-start.10
  9.2 1.6 collective-permute-start.11
  11.7 4.3 %collective-permute-done.10.refs_0_ = bf16[64,2048]{1,0:T(8,128)(2,1)S(1)} collective-permute-done((bf16[64,2048]{1,0:T(8,128)(2,1)S(1)}, bf16[64,2048]{1,0:T(8,128)(2,1)S(1)}, u32[]{:S(2)}, u32[]{:S(2)}) %collective-permute-start.10) | collective-permute-done | bytes 262176 | tf_op jit(solution)/shard_map/ppermute | solution.py:195
  15.9 2.4 %collective-permute-done.11.refs_1_ = bf16[64,2048]{1,0:T(8,128)(2,1)S(1)} collective-permute-done((bf16[64,2048]{1,0:T(8,128)(2,1)S(1)}, bf16[64,2048]{1,0:T(8,128)(2,1)S(1)}, u32[]{:S(2)}, u32[]{:S(2)}) %collective-permute-start.11) | collective-permute-done | bytes 262176 | tf_op jit(solution)/shard_map/ppermute | solution.py:195
  18.3 3.6 %collective-permute-start.30 = (bf16[64,2048]{1,0:T(8,128)(2,1)S(1)}, bf16[64,2048]{1,0:T(8,128)(2,1)S(1)}, u32[]{:S(2)}, u32[]{:S(2)}) collective-permute-start(bf16[64,2048]{1,0:T(8,128)(2,1)S(1)} %get-tuple-element.48), channel_id=1, source_target_pairs={{0,24},{4,28},{8,16},{12,20},{16,8},{20,12},{24,0},{28,4},{1,25},{... | collective-permute-start | bytes 786440 | tf_op jit(solution)/shard_map/ppermute | solution.py:195
  21.9 0.6 collective-permute-done.12.refs_2_
  22.6 12.6 %collective-permute-start.31 = (bf16[64,2048]{1,0:T(8,128)(2,1)S(1)}, bf16[64,2048]{1,0:T(8,128)(2,1)S(1)}, u32[]{:S(2)}, u32[]{:S(2)}) collective-permute-start(bf16[64,2048]{1,0:T(8,128)(2,1)S(1)} %get-tuple-element.49), channel_id=1, source_target_pairs={{0,28},{4,24},{8,20},{12,16},{16,12},{20,8},{24,4},{28,0},{1,29},{... | collective-permute-start | bytes 786440 | tf_op jit(solution)/shard_map/ppermute | solution.py:195
  35.2 8.5 %collective-permute-start.22 = (bf16[64,2048]{1,0:T(8,128)(2,1)S(1)}, bf16[64,2048]{1,0:T(8,128)(2,1)S(1)}, u32[]{:S(2)}, u32[]{:S(2)}) collective-permute-start(bf16[64,2048]{1,0:T(8,128)(2,1)S(1)} %get-tuple-element.42), channel_id=1, source_target_pairs={{0,16},{4,20},{8,24},{12,28},{16,0},{20,4},{24,8},{28,12},{1,17},{... | collective-permute-start | bytes 786440 | tf_op jit(solution)/shard_map/ppermute | solution.py:195
  43.7 12.1 %collective-permute-start.23 = (bf16[64,2048]{1,0:T(8,128)(2,1)S(1)}, bf16[64,2048]{1,0:T(8,128)(2,1)S(1)}, u32[]{:S(2)}, u32[]{:S(2)}) collective-permute-start(bf16[64,2048]{1,0:T(8,128)(2,1)S(1)} %get-tuple-element.43), channel_id=1, source_target_pairs={{0,20},{4,16},{8,28},{12,24},{16,4},{20,0},{24,12},{28,8},{1,21},{... | collective-permute-start | bytes 786440 | tf_op jit(solution)/shard_map/ppermute | solution.py:195
  55.8 5.3 %collective-permute-done.22.refs_0_ = bf16[64,2048]{1,0:T(8,128)(2,1)S(1)} collective-permute-done((bf16[64,2048]{1,0:T(8,128)(2,1)S(1)}, bf16[64,2048]{1,0:T(8,128)(2,1)S(1)}, u32[]{:S(2)}, u32[]{:S(2)}) %collective-permute-start.22) | collective-permute-done | bytes 262176 | tf_op jit(solution)/shard_map/ppermute | solution.py:195
  61.1 0.5 collective-permute-start.13
  61.7 4.3 %collective-permute-done.23.refs_1_ = bf16[64,2048]{1,0:T(8,128)(2,1)S(1)} collective-permute-done((bf16[64,2048]{1,0:T(8,128)(2,1)S(1)}, bf16[64,2048]{1,0:T(8,128)(2,1)S(1)}, u32[]{:S(2)}, u32[]{:S(2)}) %collective-permute-start.23) | collective-permute-done | bytes 262176 | tf_op jit(solution)/shard_map/ppermute | solution.py:195
  66.5 1.6 collective-permute-done.13.refs_3_
  68.1 0.5 collective-permute-start.15
  68.6 6.5 %collective-permute-done.14.refs_4_ = bf16[64,2048]{1,0:T(8,128)(2,1)S(1)} collective-permute-done((bf16[64,2048]{1,0:T(8,128)(2,1)S(1)}, bf16[64,2048]{1,0:T(8,128)(2,1)S(1)}, u32[]{:S(2)}, u32[]{:S(2)}) %collective-permute-start.14) | collective-permute-done | bytes 262176 | tf_op jit(solution)/shard_map/ppermute | solution.py:195
  75.1 0.5 collective-permute-start.32
  75.7 5.1 %collective-permute-done.15.refs_5_ = bf16[64,2048]{1,0:T(8,128)(2,1)S(1)} collective-permute-done((bf16[64,2048]{1,0:T(8,128)(2,1)S(1)}, bf16[64,2048]{1,0:T(8,128)(2,1)S(1)}, u32[]{:S(2)}, u32[]{:S(2)}) %collective-permute-start.15) | collective-permute-done | bytes 262176 | tf_op jit(solution)/shard_map/ppermute | solution.py:195
  80.7 0.5 collective-permute-start.33
  81.3 5.1 %collective-permute-done.32.refs_2_ = bf16[64,2048]{1,0:T(8,128)(2,1)S(1)} collective-permute-done((bf16[64,2048]{1,0:T(8,128)(2,1)S(1)}, bf16[64,2048]{1,0:T(8,128)(2,1)S(1)}, u32[]{:S(2)}, u32[]{:S(2)}) %collective-permute-start.32) | collective-permute-done | bytes 262176 | tf_op jit(solution)/shard_map/ppermute | solution.py:195
  86.4 0.5 collective-permute-start.24
  86.9 5.1 %collective-permute-done.33.refs_3_ = bf16[64,2048]{1,0:T(8,128)(2,1)S(1)} collective-permute-done((bf16[64,2048]{1,0:T(8,128)(2,1)S(1)}, bf16[64,2048]{1,0:T(8,128)(2,1)S(1)}, u32[]{:S(2)}, u32[]{:S(2)}) %collective-permute-start.33) | collective-permute-done | bytes 262176 | tf_op jit(solution)/shard_map/ppermute | solution.py:195
  92.0 0.5 collective-permute-start.1
  92.5 5.1 %collective-permute-done.24.refs_2_ = bf16[64,2048]{1,0:T(8,128)(2,1)S(1)} collective-permute-done((bf16[64,2048]{1,0:T(8,128)(2,1)S(1)}, bf16[64,2048]{1,0:T(8,128)(2,1)S(1)}, u32[]{:S(2)}, u32[]{:S(2)}) %collective-permute-start.24) | collective-permute-done | bytes 262176 | tf_op jit(solution)/shard_map/ppermute | solution.py:195
  98.2 0.9 slice_bitcast_fusion
  99.1 0.6 collective-permute-start.25
  99.7 1.4 copy-done
  101.1 1.4 copy-done.2
  102.5 1.4 copy-done.4
  103.9 3.6 %shard_map.179 = (bf16[64,2048]{1,0:T(8,128)(2,1)S(1)}, bf16[64,2048]{1,0:T(8,128)(2,1)S(1)}, bf16[64,2048]{1,0:T(8,128)(2,1)S(1)}, bf16[64,2048]{1,0:T(8,128)(2...) custom-call(bf16[64,2048]{1,0:T(8,128)(2,1)S(1)} %collective-permute-done.10.refs_0_, ...), custom_call_target="tpu_custom_call" | custom-call | flops 1811939328 | bytes 12582912 | tf_op jit(solution)/shard_map/pallas_call | solution.py:210
  107.5 4.9 %collective-permute-done.25.refs_3_ = bf16[64,2048]{1,0:T(8,128)(2,1)S(1)} collective-permute-done((bf16[64,2048]{1,0:T(8,128)(2,1)S(1)}, bf16[64,2048]{1,0:T(8,128)(2,1)S(1)}, u32[]{:S(2)}, u32[]{:S(2)}) %collective-permute-start.25) | collective-permute-done | bytes 262176 | tf_op jit(solution)/shard_map/ppermute | solution.py:195
  112.4 0.5 collective-permute-start.20
  113.0 3.3 %shard_map.181 = (bf16[64,2048]{1,0:T(8,128)(2,1)S(1)}, bf16[64,2048]{1,0:T(8,128)(2,1)S(1)}, bf16[64,2048]{1,0:T(8,128)(2,1)S(1)}, bf16[64,2048]{1,0:T(8,128)(2,1)S(1)}) custom-call(bf16[64,2048]{1,0:T(8,128)(2,1)S(1)} %collective-permute-done.30.refs_0_, bf16[64,2048]{1,0:T(8,128)(2,1)S(1)} %collective-permute-done.31.refs_1_, ...), custom_call_target="tpu_custom_call" | custom-call | flops 1207959552 | bytes 11534336 | tf_op jit(solution)/shard_map/pallas_call | solution.py:210
  116.3 3.3 %shard_map.180 = (bf16[64,2048]{1,0:T(8,128)(2,1)S(1)}, bf16[64,2048]{1,0:T(8,128)(2,1)S(1)}, bf16[64,2048]{1,0:T(8,128)(2,1)S(1)}, bf16[64,2048]{1,0:T(8,128)(2,1)S(1)}) custom-call(bf16[64,2048]{1,0:T(8,128)(2,1)S(1)} %collective-permute-done.22.refs_0_, bf16[64,2048]{1,0:T(8,128)(2,1)S(1)} %collective-permute-done.23.refs_1_, ...), custom_call_target="tpu_custom_call" | custom-call | flops 1207959552 | bytes 11534336 | tf_op jit(solution)/shard_map/pallas_call | solution.py:210
  119.6 1.5 collective-permute-start
  121.1 2.2 %collective-permute-start.18 = (bf16[64,2048]{1,0:T(8,128)(2,1)S(1)}, bf16[64,2048]{1,0:T(8,128)(2,1)S(1)}, u32[]{:S(2)}, u32[]{:S(2)}) collective-permute-start(bf16[64,2048]{1,0:T(8,128)(2,1)S(1)} %get-tuple-element.39), channel_id=1, source_target_pairs={{0,2},{1,3},{2,0},{3,1},{4,6},{5,7},{6,4},{7,5},{8,10},{9,11},{10,... | collective-permute-start | bytes 786440 | tf_op jit(solution)/shard_map/ppermute | solution.py:195
  123.4 1.9 collective-permute-start.36
  125.3 5.7 %shard_map.178 = (f32[128,2048]{1,0:T(8,128)S(1)}, bf16[128,2048]{1,0:T(8,128)(2,1)}) custom-call(bf16[128,2048]{1,0:T(8,128)(2,1)S(1)} %get-tuple-element.29.own_ref, bf16[128,2048]{1,0:T(8,128)(2,1)S(1)} %collective-permute-done.1.other_ref, bf16[192,128]{1,0:T(8,128)(2,1)S(1)} %get-tuple-element.30.own_tab, ...), custom_call_target="tpu_custom_call" | custom-call | flops 1409286144 | bytes 15302656 | tf_op jit(solution)/shard_map/pallas_call | solution.py:210
  131.2 2.0 collective-permute-start.28
  133.2 2.4 %collective-permute-done.16 = bf16[64,2048]{1,0:T(8,128)(2,1)S(1)} collective-permute-done((bf16[64,2048]{1,0:T(8,128)(2,1)S(1)}, bf16[64,2048]{1,0:T(8,128)(2,1)S(1)}, u32[]{:S(2)}, u32[]{:S(2)}) %collective-permute-start.16) | collective-permute-done | bytes 262176 | tf_op jit(solution)/shard_map/ppermute | solution.py:195
  135.6 2.5 %collective-permute-start.26 = (bf16[64,2048]{1,0:T(8,128)(2,1)S(1)}, bf16[64,2048]{1,0:T(8,128)(2,1)S(1)}, u32[]{:S(2)}, u32[]{:S(2)}) collective-permute-start(bf16[64,2048]{1,0:T(8,128)(2,1)S(1)} %get-tuple-element.45), channel_id=1, source_target_pairs={{0,2},{1,3},{2,0},{3,1},{4,6},{5,7},{6,4},{7,5},{8,10},{9,11},{10,... | collective-permute-start | bytes 786440 | tf_op jit(solution)/shard_map/ppermute | solution.py:195
  138.1 3.1 %collective-permute-done.36 = bf16[64,2048]{1,0:T(8,128)(2,1)S(1)} collective-permute-done((bf16[64,2048]{1,0:T(8,128)(2,1)S(1)}, bf16[64,2048]{1,0:T(8,128)(2,1)S(1)}, u32[]{:S(2)}, u32[]{:S(2)}) %collective-permute-start.36) | collective-permute-done | bytes 262176 | tf_op jit(solution)/shard_map/ppermute | solution.py:195
  141.2 2.5 %collective-permute-start.9 = (bf16[128,2048]{1,0:T(8,128)(2,1)}, bf16[128,2048]{1,0:T(8,128)(2,1)S(1)}, u32[]{:S(2)}, u32[]{:S(2)}) collective-permute-start(bf16[128,2048]{1,0:T(8,128)(2,1)} %get-tuple-element.32), channel_id=1, source_target_pairs={{0,2},{1,3},{2,0},{3,1},{4,6},{5,7},{6,4},{7,5},{8,10},{9,11},{10,... | collective-permute-start | bytes 1572872 | tf_op jit(solution)/shard_map/ppermute | solution.py:195
  143.7 0.8 add_convert_fusion
  144.5 2.3 %collective-permute-done.34 = bf16[64,2048]{1,0:T(8,128)(2,1)S(1)} collective-permute-done((bf16[64,2048]{1,0:T(8,128)(2,1)S(1)}, bf16[64,2048]{1,0:T(8,128)(2,1)S(1)}, u32[]{:S(2)}, u32[]{:S(2)}) %collective-permute-start.34) | collective-permute-done | bytes 262176 | tf_op jit(solution)/shard_map/ppermute | solution.py:195
  146.8 1.1 collective-permute-start.21
  147.9 0.8 add_convert_fusion.1
  148.7 3.7 %collective-permute-done.28 = bf16[64,2048]{1,0:T(8,128)(2,1)S(1)} collective-permute-done((bf16[64,2048]{1,0:T(8,128)(2,1)S(1)}, bf16[64,2048]{1,0:T(8,128)(2,1)S(1)}, u32[]{:S(2)}, u32[]{:S(2)}) %collective-permute-start.28) | collective-permute-done | bytes 262176 | tf_op jit(solution)/shard_map/ppermute | solution.py:195
  152.4 0.8 add_convert_fusion.2
  153.2 4.8 %collective-permute-done.26 = bf16[64,2048]{1,0:T(8,128)(2,1)S(1)} collective-permute-done((bf16[64,2048]{1,0:T(8,128)(2,1)S(1)}, bf16[64,2048]{1,0:T(8,128)(2,1)S(1)}, u32[]{:S(2)}, u32[]{:S(2)}) %collective-permute-start.26) | collective-permute-done | bytes 262176 | tf_op jit(solution)/shard_map/ppermute | solution.py:195
  158.1 1.8 collective-permute-start.17
  159.9 0.8 add_convert_fusion.3
  160.7 3.7 %collective-permute-start.37 = (bf16[64,2048]{1,0:T(8,128)(2,1)}, bf16[64,2048]{1,0:T(8,128)(2,1)S(1)}, u32[]{:S(2)}, u32[]{:S(2)}) collective-permute-start(bf16[64,2048]{1,0:T(8,128)(2,1)} %add_convert_fusion), channel_id=1, source_target_pairs={{0,28},{4,24},{8,20},{12,16},{16,12},{20,8},{24,4},{28,0},{1,29},{... | collective-permute-start | bytes 786440 | tf_op jit(solution)/shard_map/ppermute | solution.py:195
  165.2 3.5 %collective-permute-start.27 = (bf16[64,2048]{1,0:T(8,128)(2,1)}, bf16[64,2048]{1,0:T(8,128)(2,1)}, u32[]{:S(2)}, u32[]{:S(2)}) collective-permute-start(bf16[64,2048]{1,0:T(8,128)(2,1)} %add_convert_fusion.3), channel_id=1, source_target_pairs={{0,16},{4,20},{8,24},{12,28},{16,0},{20,4},{24,8},{28,12},{1,17},{... | collective-permute-start | bytes 786440 | tf_op jit(solution)/shard_map/ppermute | solution.py:195
  168.7 2.2 %copy-done.6 = bf16[1024,2048]{1,0:T(8,128)(2,1)S(1)} copy-done((bf16[1024,2048]{1,0:T(8,128)(2,1)S(1)}, bf16[1024,2048]{1,0:T(8,128)(2,1)}, u32[]{:S(2)}) %copy-start.6) | copy-done | bytes 4194328
  170.9 9.4 %shard_map.176 = bf16[256,2048]{1,0:T(8,128)(2,1)} custom-call(bf16[256,1024]{1,0:T(8,128)(2,1)S(1)} %copy-done.7, bf16[256,256]{1,0:T(8,128)(2,1)S(1)} %copy-done.11, bf16[256,256]{1,0:T(8,128)(2,1)S(1)} %copy-done.12, bf16[2,128,256]{2,1,0:T(8,128)(2,1)S(1)} %collective-permute-done.rim_ref, f32[16]{0:T(128)S(1)} %copy-done.17, s32[1]{0:T(128)} %bitcast.2.first_ref, ...), custom_call_target="tpu_custom_call" | custom-call | flops 1610612736 | bytes 5767168 | tf_op jit(solution)/shard_map/pallas_call | solution.py:106
  180.3 23.8 %collective-permute-done.29.refs_4_ = bf16[64,2048]{1,0:T(8,128)(2,1)} collective-permute-done((bf16[64,2048]{1,0:T(8,128)(2,1)}, bf16[64,2048]{1,0:T(8,128)(2,1)}, u32[]{:S(2)}, u32[]{:S(2)}) %collective-permute-start.29) | collective-permute-done | bytes 262176 | tf_op jit(solution)/shard_map/ppermute | solution.py:195
  204.1 2.6 %collective-permute-done.27.refs_3_ = bf16[64,2048]{1,0:T(8,128)(2,1)} collective-permute-done((bf16[64,2048]{1,0:T(8,128)(2,1)}, bf16[64,2048]{1,0:T(8,128)(2,1)}, u32[]{:S(2)}, u32[]{:S(2)}) %collective-permute-start.27) | collective-permute-done | bytes 262176 | tf_op jit(solution)/shard_map/ppermute | solution.py:195
  206.7 2.8 %shard_map.182 = bf16[128,2048]{1,0:T(8,128)(2,1)} custom-call(s32[2,128]{1,0:T(2,128)S(1)} %get-tuple-element.28.slot_ref, f32[2,128]{1,0:T(2,128)S(1)} %bitcast.38, f32[128,2048]{1,0:T(8,128)S(1)} %get-tuple-element.31.shared_ref, bf16[128,2048]{1,0:T(8,128)(2,1)S(1)} %collective-permute-done.9.back_ref, f32[1,2048]{1,0:T(1,128)S(1)} %bitcast.36, ...), custom_call_target="tpu_custom_call" | custom-call | flops 469762048 | bytes 3942400 | tf_op jit(solution)/shard_map/pallas_call | solution.py:210
  (69 shorter events, 3.3 us)
Async XLA Ops:
  1.3 0.7 copy-start.15
  2.0 1.0 copy-start.18
  3.1 0.7 copy-start.19
  4.6 6.5 %collective-permute-start.2 = (bf16[192,128]{1,0:T(8,128)(2,1)S(1)}, bf16[192,128]{1,0:T(8,128)(2,1)S(1)}, u32[]{:S(2)}, u32[]{:S(2)}) collective-permute-start(bf16[192,128]{1,0:T(8,128)(2,1)S(1)} %get-tuple-element.30.own_tab), channel_id=1, source_target_pairs={{0,2},{1,3},{2,0},{3,1},{4,6},{5,7},{6,4},{7,5},{8,10},{9,11},{10,... | collective-permute-start | bytes 147464 | tf_op jit(solution)/shard_map/ppermute | solution.py:195
  7.6 8.3 %collective-permute-start.10 = (bf16[64,2048]{1,0:T(8,128)(2,1)S(1)}, bf16[64,2048]{1,0:T(8,128)(2,1)S(1)}, u32[]{:S(2)}, u32[]{:S(2)}) collective-permute-start(bf16[64,2048]{1,0:T(8,128)(2,1)S(1)} %get-tuple-element.33), channel_id=1, source_target_pairs={{0,4},{4,0},{8,12},{12,8},{16,20},{20,16},{24,28},{28,24},{1,5},{5... | collective-permute-start | bytes 786440 | tf_op jit(solution)/shard_map/ppermute | solution.py:195
  9.2 9.2 %collective-permute-start.11 = (bf16[64,2048]{1,0:T(8,128)(2,1)S(1)}, bf16[64,2048]{1,0:T(8,128)(2,1)S(1)}, u32[]{:S(2)}, u32[]{:S(2)}) collective-permute-start(bf16[64,2048]{1,0:T(8,128)(2,1)S(1)} %get-tuple-element.34), channel_id=1, source_target_pairs={{0,8},{4,12},{8,0},{12,4},{16,24},{20,28},{24,16},{28,20},{1,9},{5... | collective-permute-start | bytes 786440 | tf_op jit(solution)/shard_map/ppermute | solution.py:195
  10.7 11.8 %collective-permute-start.12 = (bf16[64,2048]{1,0:T(8,128)(2,1)S(1)}, bf16[64,2048]{1,0:T(8,128)(2,1)S(1)}, u32[]{:S(2)}, u32[]{:S(2)}) collective-permute-start(bf16[64,2048]{1,0:T(8,128)(2,1)S(1)} %get-tuple-element.35), channel_id=1, source_target_pairs={{0,12},{4,8},{8,4},{12,0},{16,28},{20,24},{24,20},{28,16},{1,13},{... | collective-permute-start | bytes 786440 | tf_op jit(solution)/shard_map/ppermute | solution.py:195
  11.1 86.5 %collective-permute-start.6 = (bf16[2,192,2048]{2,1,0:T(8,128)(2,1)}, bf16[2,192,2048]{2,1,0:T(8,128)(2,1)S(1)}, u32[]{:S(2)}, u32[]{:S(2)}) collective-permute-start(bf16[2,192,2048]{2,1,0:T(8,128)(2,1)} %bitcast.25), channel_id=1, source_target_pairs={{0,1},{1,0},{2,3},{3,2},{4,5},{5,4},{6,7},{7,6},{8,9},{9,8},{10,11... | collective-permute-start | bytes 4718600 | tf_op jit(solution)/shard_map/ppermute | solution.py:195
  11.1 87.0 %collective-permute-start.7 = (bf16[2,192,2048]{2,1,0:T(8,128)(2,1)}, bf16[2,192,2048]{2,1,0:T(8,128)(2,1)S(1)}, u32[]{:S(2)}, u32[]{:S(2)}) collective-permute-start(bf16[2,192,2048]{2,1,0:T(8,128)(2,1)} %bitcast.30), channel_id=1, source_target_pairs={{0,1},{1,0},{2,3},{3,2},{4,5},{5,4},{6,7},{7,6},{8,9},{9,8},{10,11... | collective-permute-start | bytes 4718600 | tf_op jit(solution)/shard_map/ppermute | solution.py:195
  15.9 83.1 %collective-permute-start.8 = (bf16[2,192,2048]{2,1,0:T(8,128)(2,1)}, bf16[2,192,2048]{2,1,0:T(8,128)(2,1)S(1)}, u32[]{:S(2)}, u32[]{:S(2)}) collective-permute-start(bf16[2,192,2048]{2,1,0:T(8,128)(2,1)} %refs_8_.3), channel_id=1, source_target_pairs={{0,1},{1,0},{2,3},{3,2},{4,5},{5,4},{6,7},{7,6},{8,9},{9,8},{10,11... | collective-permute-start | bytes 4718600 | tf_op jit(solution)/shard_map/ppermute | solution.py:195
  18.3 16.9 %collective-permute-start.30 = (bf16[64,2048]{1,0:T(8,128)(2,1)S(1)}, bf16[64,2048]{1,0:T(8,128)(2,1)S(1)}, u32[]{:S(2)}, u32[]{:S(2)}) collective-permute-start(bf16[64,2048]{1,0:T(8,128)(2,1)S(1)} %get-tuple-element.48), channel_id=1, source_target_pairs={{0,24},{4,28},{8,16},{12,20},{16,8},{20,12},{24,0},{28,4},{1,25},{... | collective-permute-start | bytes 786440 | tf_op jit(solution)/shard_map/ppermute | solution.py:195
  22.6 21.1 %collective-permute-start.31 = (bf16[64,2048]{1,0:T(8,128)(2,1)S(1)}, bf16[64,2048]{1,0:T(8,128)(2,1)S(1)}, u32[]{:S(2)}, u32[]{:S(2)}) collective-permute-start(bf16[64,2048]{1,0:T(8,128)(2,1)S(1)} %get-tuple-element.49), channel_id=1, source_target_pairs={{0,28},{4,24},{8,20},{12,16},{16,12},{20,8},{24,4},{28,0},{1,29},{... | collective-permute-start | bytes 786440 | tf_op jit(solution)/shard_map/ppermute | solution.py:195
  35.2 25.9 %collective-permute-start.22 = (bf16[64,2048]{1,0:T(8,128)(2,1)S(1)}, bf16[64,2048]{1,0:T(8,128)(2,1)S(1)}, u32[]{:S(2)}, u32[]{:S(2)}) collective-permute-start(bf16[64,2048]{1,0:T(8,128)(2,1)S(1)} %get-tuple-element.42), channel_id=1, source_target_pairs={{0,16},{4,20},{8,24},{12,28},{16,0},{20,4},{24,8},{28,12},{1,17},{... | collective-permute-start | bytes 786440 | tf_op jit(solution)/shard_map/ppermute | solution.py:195
  43.7 22.3 %collective-permute-start.23 = (bf16[64,2048]{1,0:T(8,128)(2,1)S(1)}, bf16[64,2048]{1,0:T(8,128)(2,1)S(1)}, u32[]{:S(2)}, u32[]{:S(2)}) collective-permute-start(bf16[64,2048]{1,0:T(8,128)(2,1)S(1)} %get-tuple-element.43), channel_id=1, source_target_pairs={{0,20},{4,16},{8,28},{12,24},{16,4},{20,0},{24,12},{28,8},{1,21},{... | collective-permute-start | bytes 786440 | tf_op jit(solution)/shard_map/ppermute | solution.py:195
  61.1 6.9 %collective-permute-start.13 = (bf16[64,2048]{1,0:T(8,128)(2,1)S(1)}, bf16[64,2048]{1,0:T(8,128)(2,1)S(1)}, u32[]{:S(2)}, u32[]{:S(2)}) collective-permute-start(bf16[64,2048]{1,0:T(8,128)(2,1)S(1)} %collective-permute-done.10.refs_0_), channel_id=1, source_target_pairs={{0,2},{1,3},{2,0},{3,1},{4,6},{5,7},{6,4},{7,5},{8,10},{9,11},{10,... | collective-permute-start | bytes 786440 | tf_op jit(solution)/shard_map/ppermute | solution.py:195
  65.9 9.2 %collective-permute-start.14 = (bf16[64,2048]{1,0:T(8,128)(2,1)S(1)}, bf16[64,2048]{1,0:T(8,128)(2,1)S(1)}, u32[]{:S(2)}, u32[]{:S(2)}) collective-permute-start(bf16[64,2048]{1,0:T(8,128)(2,1)S(1)} %collective-permute-done.11.refs_1_), channel_id=1, source_target_pairs={{0,2},{1,3},{2,0},{3,1},{4,6},{5,7},{6,4},{7,5},{8,10},{9,11},{10,... | collective-permute-start | bytes 786440 | tf_op jit(solution)/shard_map/ppermute | solution.py:195
  68.1 12.7 %collective-permute-start.15 = (bf16[64,2048]{1,0:T(8,128)(2,1)S(1)}, bf16[64,2048]{1,0:T(8,128)(2,1)S(1)}, u32[]{:S(2)}, u32[]{:S(2)}) collective-permute-start(bf16[64,2048]{1,0:T(8,128)(2,1)S(1)} %collective-permute-done.12.refs_2_), channel_id=1, source_target_pairs={{0,2},{1,3},{2,0},{3,1},{4,6},{5,7},{6,4},{7,5},{8,10},{9,11},{10,... | collective-permute-start | bytes 786440 | tf_op jit(solution)/shard_map/ppermute | solution.py:195
  75.1 11.2 %collective-permute-start.32 = (bf16[64,2048]{1,0:T(8,128)(2,1)S(1)}, bf16[64,2048]{1,0:T(8,128)(2,1)S(1)}, u32[]{:S(2)}, u32[]{:S(2)}) collective-permute-start(bf16[64,2048]{1,0:T(8,128)(2,1)S(1)} %collective-permute-done.30.refs_0_), channel_id=1, source_target_pairs={{0,2},{1,3},{2,0},{3,1},{4,6},{5,7},{6,4},{7,5},{8,10},{9,11},{10,... | collective-permute-start | bytes 786440 | tf_op jit(solution)/shard_map/ppermute | solution.py:195
  80.7 11.2 %collective-permute-start.33 = (bf16[64,2048]{1,0:T(8,128)(2,1)S(1)}, bf16[64,2048]{1,0:T(8,128)(2,1)S(1)}, u32[]{:S(2)}, u32[]{:S(2)}) collective-permute-start(bf16[64,2048]{1,0:T(8,128)(2,1)S(1)} %collective-permute-done.31.refs_1_), channel_id=1, source_target_pairs={{0,2},{1,3},{2,0},{3,1},{4,6},{5,7},{6,4},{7,5},{8,10},{9,11},{10,... | collective-permute-start | bytes 786440 | tf_op jit(solution)/shard_map/ppermute | solution.py:195
  86.4 11.2 %collective-permute-start.24 = (bf16[64,2048]{1,0:T(8,128)(2,1)S(1)}, bf16[64,2048]{1,0:T(8,128)(2,1)S(1)}, u32[]{:S(2)}, u32[]{:S(2)}) collective-permute-start(bf16[64,2048]{1,0:T(8,128)(2,1)S(1)} %collective-permute-done.22.refs_0_), channel_id=1, source_target_pairs={{0,2},{1,3},{2,0},{3,1},{4,6},{5,7},{6,4},{7,5},{8,10},{9,11},{10,... | collective-permute-start | bytes 786440 | tf_op jit(solution)/shard_map/ppermute | solution.py:195
  92.0 27.6 %collective-permute-start.1 = (bf16[128,2048]{1,0:T(8,128)(2,1)S(1)}, bf16[128,2048]{1,0:T(8,128)(2,1)S(1)}, u32[]{:S(2)}, u32[]{:S(2)}) collective-permute-start(bf16[128,2048]{1,0:T(8,128)(2,1)S(1)} %get-tuple-element.29.own_ref), channel_id=1, source_target_pairs={{0,2},{1,3},{2,0},{3,1},{4,6},{5,7},{6,4},{7,5},{8,10},{9,11},{10,... | collective-permute-start | bytes 1572872 | tf_op jit(solution)/shard_map/ppermute | solution.py:195
  97.6 23.5 %collective-permute-start.3 = (bf16[2048,128]{1,0:T(8,128)(2,1)}, bf16[2048,128]{1,0:T(8,128)(2,1)S(1)}, u32[]{:S(2)}, u32[]{:S(2)}) collective-permute-start(bf16[2048,128]{1,0:T(8,128)(2,1)} %refs_0_.1), channel_id=1, source_target_pairs={{0,1},{1,0},{2,3},{3,2},{4,5},{5,4},{6,7},{7,6},{8,9},{9,8},{10,11... | collective-permute-start | bytes 1572872 | tf_op jit(solution)/shard_map/ppermute | solution.py:195
  97.6 25.7 %collective-permute-start.4 = (bf16[2048,128]{1,0:T(8,128)(2,1)}, bf16[2048,128]{1,0:T(8,128)(2,1)S(1)}, u32[]{:S(2)}, u32[]{:S(2)}) collective-permute-start(bf16[2048,128]{1,0:T(8,128)(2,1)} %refs_2_.1), channel_id=1, source_target_pairs={{0,1},{1,0},{2,3},{3,2},{4,5},{5,4},{6,7},{7,6},{8,9},{9,8},{10,11... | collective-permute-start | bytes 1572872 | tf_op jit(solution)/shard_map/ppermute | solution.py:195
  98.1 25.3 %collective-permute-start.5 = (bf16[128,2048]{1,0:T(8,128)(2,1)}, bf16[128,2048]{1,0:T(8,128)(2,1)S(1)}, u32[]{:S(2)}, u32[]{:S(2)}) collective-permute-start(bf16[128,2048]{1,0:T(8,128)(2,1)} %refs_4_.1), channel_id=1, source_target_pairs={{0,1},{1,0},{2,3},{3,2},{4,5},{5,4},{6,7},{7,6},{8,9},{9,8},{10,11... | collective-permute-start | bytes 1572872 | tf_op jit(solution)/shard_map/ppermute | solution.py:195
  99.1 13.4 %collective-permute-start.25 = (bf16[64,2048]{1,0:T(8,128)(2,1)S(1)}, bf16[64,2048]{1,0:T(8,128)(2,1)S(1)}, u32[]{:S(2)}, u32[]{:S(2)}) collective-permute-start(bf16[64,2048]{1,0:T(8,128)(2,1)S(1)} %collective-permute-done.23.refs_1_), channel_id=1, source_target_pairs={{0,2},{1,3},{2,0},{3,1},{4,6},{5,7},{6,4},{7,5},{8,10},{9,11},{10,... | collective-permute-start | bytes 786440 | tf_op jit(solution)/shard_map/ppermute | solution.py:195
  99.7 1.4 copy-start
  101.1 1.4 copy-start.2
  102.5 1.4 copy-start.4
  112.4 18.6 %collective-permute-start.20 = (bf16[64,2048]{1,0:T(8,128)(2,1)S(1)}, bf16[64,2048]{1,0:T(8,128)(2,1)S(1)}, u32[]{:S(2)}, u32[]{:S(2)}) collective-permute-start(bf16[64,2048]{1,0:T(8,128)(2,1)S(1)} %get-tuple-element.41), channel_id=1, source_target_pairs={{0,2},{1,3},{2,0},{3,1},{4,6},{5,7},{6,4},{7,5},{8,10},{9,11},{10,... | collective-permute-start | bytes 786440 | tf_op jit(solution)/shard_map/ppermute | solution.py:195
  116.2 9.1 %copy-start.1 = (bf16[2,2048,192]{1,2,0:T(8,128)(2,1)S(1)}, bf16[2,2048,192]{1,2,0:T(8,128)(2,1)}, u32[]{:S(2)}) copy-start(bf16[2,2048,192]{1,2,0:T(8,128)(2,1)} %param.27) | copy-start | bytes 4718596
  116.3 9.1 %copy-start.3 = (bf16[2,2048,192]{1,2,0:T(8,128)(2,1)S(1)}, bf16[2,2048,192]{1,2,0:T(8,128)(2,1)}, u32[]{:S(2)}) copy-start(bf16[2,2048,192]{1,2,0:T(8,128)(2,1)} %param.28) | copy-start | bytes 4718596
  116.3 9.0 %copy-start.5 = (bf16[2,192,2048]{2,1,0:T(8,128)(2,1)S(1)}, bf16[2,192,2048]{2,1,0:T(8,128)(2,1)}, u32[]{:S(2)}) copy-start(bf16[2,192,2048]{2,1,0:T(8,128)(2,1)} %refs_8_.3) | copy-start | bytes 4718596
  116.3 9.0 %copy-start.8 = (bf16[2048,128]{1,0:T(8,128)(2,1)S(1)}, bf16[2048,128]{1,0:T(8,128)(2,1)}, u32[]{:S(2)}) copy-start(bf16[2048,128]{1,0:T(8,128)(2,1)} %refs_0_.1) | copy-start | bytes 1572868
  116.3 9.0 %copy-start.9 = (bf16[2048,128]{1,0:T(8,128)(2,1)S(1)}, bf16[2048,128]{1,0:T(8,128)(2,1)}, u32[]{:S(2)}) copy-start(bf16[2048,128]{1,0:T(8,128)(2,1)} %refs_2_.1) | copy-start | bytes 1572868
  116.3 9.0 %copy-start.10 = (bf16[128,2048]{1,0:T(8,128)(2,1)S(1)}, bf16[128,2048]{1,0:T(8,128)(2,1)}, u32[]{:S(2)}) copy-start(bf16[128,2048]{1,0:T(8,128)(2,1)} %refs_4_.1) | copy-start | bytes 1572868
  119.6 41.1 %collective-permute-start = (bf16[2,128,256]{2,1,0:T(8,128)(2,1)S(1)}, bf16[2,128,256]{2,1,0:T(8,128)(2,1)S(1)}, u32[]{:S(2)}, u32[]{:S(2)}) collective-permute-start(bf16[2,128,256]{2,1,0:T(8,128)(2,1)S(1)} %pad_maximum_fusion), channel_id=1, source_target_pairs={{0,1},{1,2},{2,3},{3,4},{4,5},{5,6},{6,7},{7,8},{8,9},{9,10},{10,1... | collective-permute-start | bytes 393224 | tf_op jit(solution)/shard_map/ppermute | solution.py:26
  121.1 10.1 %collective-permute-start.18 = (bf16[64,2048]{1,0:T(8,128)(2,1)S(1)}, bf16[64,2048]{1,0:T(8,128)(2,1)S(1)}, u32[]{:S(2)}, u32[]{:S(2)}) collective-permute-start(bf16[64,2048]{1,0:T(8,128)(2,1)S(1)} %get-tuple-element.39), channel_id=1, source_target_pairs={{0,2},{1,3},{2,0},{3,1},{4,6},{5,7},{6,4},{7,5},{8,10},{9,11},{10,... | collective-permute-start | bytes 786440 | tf_op jit(solution)/shard_map/ppermute | solution.py:195
  123.3 12.3 %collective-permute-start.16 = (bf16[64,2048]{1,0:T(8,128)(2,1)S(1)}, bf16[64,2048]{1,0:T(8,128)(2,1)S(1)}, u32[]{:S(2)}, u32[]{:S(2)}) collective-permute-start(bf16[64,2048]{1,0:T(8,128)(2,1)S(1)} %get-tuple-element.37), channel_id=1, source_target_pairs={{0,2},{1,3},{2,0},{3,1},{4,6},{5,7},{6,4},{7,5},{8,10},{9,11},{10,... | collective-permute-start | bytes 786440 | tf_op jit(solution)/shard_map/ppermute | solution.py:195
  123.4 17.8 %collective-permute-start.36 = (bf16[64,2048]{1,0:T(8,128)(2,1)S(1)}, bf16[64,2048]{1,0:T(8,128)(2,1)S(1)}, u32[]{:S(2)}, u32[]{:S(2)}) collective-permute-start(bf16[64,2048]{1,0:T(8,128)(2,1)S(1)} %get-tuple-element.53), channel_id=1, source_target_pairs={{0,2},{1,3},{2,0},{3,1},{4,6},{5,7},{6,4},{7,5},{8,10},{9,11},{10,... | collective-permute-start | bytes 786440 | tf_op jit(solution)/shard_map/ppermute | solution.py:195
  131.0 15.8 %collective-permute-start.34 = (bf16[64,2048]{1,0:T(8,128)(2,1)S(1)}, bf16[64,2048]{1,0:T(8,128)(2,1)S(1)}, u32[]{:S(2)}, u32[]{:S(2)}) collective-permute-start(bf16[64,2048]{1,0:T(8,128)(2,1)S(1)} %get-tuple-element.51), channel_id=1, source_target_pairs={{0,2},{1,3},{2,0},{3,1},{4,6},{5,7},{6,4},{7,5},{8,10},{9,11},{10,... | collective-permute-start | bytes 786440 | tf_op jit(solution)/shard_map/ppermute | solution.py:195
  131.2 21.3 %collective-permute-start.28 = (bf16[64,2048]{1,0:T(8,128)(2,1)S(1)}, bf16[64,2048]{1,0:T(8,128)(2,1)S(1)}, u32[]{:S(2)}, u32[]{:S(2)}) collective-permute-start(bf16[64,2048]{1,0:T(8,128)(2,1)S(1)} %get-tuple-element.47), channel_id=1, source_target_pairs={{0,2},{1,3},{2,0},{3,1},{4,6},{5,7},{6,4},{7,5},{8,10},{9,11},{10,... | collective-permute-start | bytes 786440 | tf_op jit(solution)/shard_map/ppermute | solution.py:195
  135.6 22.5 %collective-permute-start.26 = (bf16[64,2048]{1,0:T(8,128)(2,1)S(1)}, bf16[64,2048]{1,0:T(8,128)(2,1)S(1)}, u32[]{:S(2)}, u32[]{:S(2)}) collective-permute-start(bf16[64,2048]{1,0:T(8,128)(2,1)S(1)} %get-tuple-element.45), channel_id=1, source_target_pairs={{0,2},{1,3},{2,0},{3,1},{4,6},{5,7},{6,4},{7,5},{8,10},{9,11},{10,... | collective-permute-start | bytes 786440 | tf_op jit(solution)/shard_map/ppermute | solution.py:195
  141.2 65.5 %collective-permute-start.9 = (bf16[128,2048]{1,0:T(8,128)(2,1)}, bf16[128,2048]{1,0:T(8,128)(2,1)S(1)}, u32[]{:S(2)}, u32[]{:S(2)}) collective-permute-start(bf16[128,2048]{1,0:T(8,128)(2,1)} %get-tuple-element.32), channel_id=1, source_target_pairs={{0,2},{1,3},{2,0},{3,1},{4,6},{5,7},{6,4},{7,5},{8,10},{9,11},{10,... | collective-permute-start | bytes 1572872 | tf_op jit(solution)/shard_map/ppermute | solution.py:195
  143.7 25.0 %copy-start.7 = (bf16[256,1024]{1,0:T(8,128)(2,1)S(1)}, bf16[256,1024]{1,0:T(8,128)(2,1)}, u32[]{:S(2)}) copy-start(bf16[256,1024]{1,0:T(8,128)(2,1)} %q_ref.1) | copy-start | bytes 1572868
  143.7 25.0 %copy-start.11 = (bf16[256,256]{1,0:T(8,128)(2,1)S(1)}, bf16[256,256]{1,0:T(8,128)(2,1)}, u32[]{:S(2)}) copy-start(bf16[256,256]{1,0:T(8,128)(2,1)} %k_ref.1) | copy-start | bytes 393220
  143.7 25.0 %copy-start.12 = (bf16[256,256]{1,0:T(8,128)(2,1)S(1)}, bf16[256,256]{1,0:T(8,128)(2,1)}, u32[]{:S(2)}) copy-start(bf16[256,256]{1,0:T(8,128)(2,1)} %v_ref.1) | copy-start | bytes 393220
  143.7 25.0 %copy-start.13 = (f32[2048]{0:T(1024)S(1)}, f32[2048]{0:T(1024)}, u32[]{:S(2)}) copy-start(f32[2048]{0:T(1024)} %param.22) | copy-start | bytes 24580
  143.7 25.0 %copy-start.17 = (f32[16]{0:T(128)S(1)}, f32[16]{0:T(128)}, u32[]{:S(2)}) copy-start(f32[16]{0:T(128)} %sink_ref.1) | copy-start | bytes 196
  146.8 17.6 %collective-permute-start.21 = (bf16[64,2048]{1,0:T(8,128)(2,1)S(1)}, bf16[64,2048]{1,0:T(8,128)(2,1)S(1)}, u32[]{:S(2)}, u32[]{:S(2)}) collective-permute-start(bf16[64,2048]{1,0:T(8,128)(2,1)S(1)} %add_convert_fusion.4), channel_id=1, source_target_pairs={{0,12},{4,8},{8,4},{12,0},{16,28},{20,24},{24,20},{28,16},{1,13},{... | collective-permute-start | bytes 786440 | tf_op jit(solution)/shard_map/ppermute | solution.py:195
  152.4 12.4 %collective-permute-start.19 = (bf16[64,2048]{1,0:T(8,128)(2,1)S(1)}, bf16[64,2048]{1,0:T(8,128)(2,1)S(1)}, u32[]{:S(2)}, u32[]{:S(2)}) collective-permute-start(bf16[64,2048]{1,0:T(8,128)(2,1)S(1)} %add_convert_fusion.5), channel_id=1, source_target_pairs={{0,8},{4,12},{8,0},{12,4},{16,24},{20,28},{24,16},{28,20},{1,9},{5... | collective-permute-start | bytes 786440 | tf_op jit(solution)/shard_map/ppermute | solution.py:195
  158.1 7.1 %collective-permute-start.17 = (bf16[64,2048]{1,0:T(8,128)(2,1)S(1)}, bf16[64,2048]{1,0:T(8,128)(2,1)S(1)}, u32[]{:S(2)}, u32[]{:S(2)}) collective-permute-start(bf16[64,2048]{1,0:T(8,128)(2,1)S(1)} %add_convert_fusion.6), channel_id=1, source_target_pairs={{0,4},{4,0},{8,12},{12,8},{16,20},{20,16},{24,28},{28,24},{1,5},{5... | collective-permute-start | bytes 786440 | tf_op jit(solution)/shard_map/ppermute | solution.py:195
  160.7 19.6 %collective-permute-start.37 = (bf16[64,2048]{1,0:T(8,128)(2,1)}, bf16[64,2048]{1,0:T(8,128)(2,1)S(1)}, u32[]{:S(2)}, u32[]{:S(2)}) collective-permute-start(bf16[64,2048]{1,0:T(8,128)(2,1)} %add_convert_fusion), channel_id=1, source_target_pairs={{0,28},{4,24},{8,20},{12,16},{16,12},{20,8},{24,4},{28,0},{1,29},{... | collective-permute-start | bytes 786440 | tf_op jit(solution)/shard_map/ppermute | solution.py:195
  164.4 15.9 %collective-permute-start.35 = (bf16[64,2048]{1,0:T(8,128)(2,1)}, bf16[64,2048]{1,0:T(8,128)(2,1)}, u32[]{:S(2)}, u32[]{:S(2)}) collective-permute-start(bf16[64,2048]{1,0:T(8,128)(2,1)} %add_convert_fusion.1), channel_id=1, source_target_pairs={{0,24},{4,28},{8,16},{12,20},{16,8},{20,12},{24,0},{28,4},{1,25},{... | collective-permute-start | bytes 786440 | tf_op jit(solution)/shard_map/ppermute | solution.py:195
  164.8 39.3 %collective-permute-start.29 = (bf16[64,2048]{1,0:T(8,128)(2,1)}, bf16[64,2048]{1,0:T(8,128)(2,1)}, u32[]{:S(2)}, u32[]{:S(2)}) collective-permute-start(bf16[64,2048]{1,0:T(8,128)(2,1)} %add_convert_fusion.2), channel_id=1, source_target_pairs={{0,20},{4,16},{8,28},{12,24},{16,4},{20,0},{24,12},{28,8},{1,21},{... | collective-permute-start | bytes 786440 | tf_op jit(solution)/shard_map/ppermute | solution.py:195
  165.2 41.6 %collective-permute-start.27 = (bf16[64,2048]{1,0:T(8,128)(2,1)}, bf16[64,2048]{1,0:T(8,128)(2,1)}, u32[]{:S(2)}, u32[]{:S(2)}) collective-permute-start(bf16[64,2048]{1,0:T(8,128)(2,1)} %add_convert_fusion.3), channel_id=1, source_target_pairs={{0,16},{4,20},{8,24},{12,28},{16,0},{20,4},{24,8},{28,12},{1,17},{... | collective-permute-start | bytes 786440 | tf_op jit(solution)/shard_map/ppermute | solution.py:195
  168.7 2.2 %copy-start.6 = (bf16[1024,2048]{1,0:T(8,128)(2,1)S(1)}, bf16[1024,2048]{1,0:T(8,128)(2,1)}, u32[]{:S(2)}) copy-start(bf16[1024,2048]{1,0:T(8,128)(2,1)} %weight_ref.1) | copy-start | bytes 12582916
  170.9 35.9 %copy-start.14 = (f32[2048]{0:T(1024)S(1)}, f32[2048]{0:T(1024)}, u32[]{:S(2)}) copy-start(f32[2048]{0:T(1024)} %param.33) | copy-start | bytes 24580
  170.9 35.9 %copy-start.16 = (f32[128,2]{0,1:T(2,128)S(1)}, f32[128,2]{0,1:T(2,128)}, u32[]{:S(2)}) copy-start(f32[128,2]{0,1:T(2,128)} %param.26) | copy-start | bytes 3076
